TPU v7x, 256 devices: a whole 4x4x8 slice. The times are simulated.
256 devices in a mesh: ep: 16 (over y, x), tp: 16 (over z, core).
Axes of the slice: x: 4, y: 4, z: 8, core: 2. Of those that a mesh axis runs over, the one named last changes fastest.
Arguments:
- tokens: bfloat16 [256, 4096], P('ep'), may hold values from -6 to 6
- attn_gain: float32 [4096], replicated, may hold values from 0.1 to 1.9
- w_query: bfloat16 [4096, 2048], P('ep', 'tp'), may hold values from -0.15625 to 0.15625
- w_key: bfloat16 [4096, 2048], P('ep', 'tp'), may hold values from -0.09375 to 0.09375
- w_value: bfloat16 [4096, 2048], P('ep', 'tp'), may hold values from -0.09375 to 0.09375
- mix_lambda: float32 [16], P('tp'), may hold values from 0.3 to 0.8
- head_gain: float32 [128], replicated, may hold values from 0.1 to 1.9
- w_output: bfloat16 [2048, 4096], P('tp'), may hold values from -0.125 to 0.125
- cache_keys: bfloat16 [256, 1024, 2048], P('ep', None, 'tp'), may hold values from -180 to 180
- cache_value: bfloat16 [256, 1024, 2048], P('ep', None, 'tp'), may hold values from -6 to 6
- lengths: int32 [256], P('ep'), may hold values from 1 to 1024
- moe_gain: float32 [4096], replicated, may hold values from 0.1 to 1.9
- group_ids: int32 [256], P('ep'), may hold values from 0 to 7, as said below
- member_ids: int32 [256, 2], P('ep'), may hold values from 0 to 1, as said below
- group_gate: float32 [256], P('ep'), may hold values from 0.3 to 1
- member_logits: float32 [256, 2], P('ep'), may hold values from -4 to 4
- w_exp_gate: bfloat16 [16, 4096, 2048], P('ep', None, 'tp'), may hold values from -0.09375 to 0.09375
- w_exp_up: bfloat16 [16, 4096, 2048], P('ep', None, 'tp'), may hold values from -0.09375 to 0.09375
- w_exp_down: bfloat16 [16, 2048, 4096], P('ep', 'tp'), may hold values from -0.125 to 0.125
Outputs:
- mixed: bfloat16 [256, 4096], P('ep', 'tp')
- fresh_keys: bfloat16 [256, 2048], P('ep', 'tp')
- fresh_value: bfloat16 [256, 2048], P('ep', 'tp')
Inputs may be any that keep to these rules, and one draw needn't show every extreme that they name: `group_ids`: each index of ep holds 16 consecutive tokens, of which every group gets the same number. A token's 2 members differ, and every expert group_ids * 2 + member_ids receives exactly 2 of the token-expert pairs of each index of ep.
All inputs are finite; a program needn't handle non-finite values.
Results may differ from a plain program's by a relative error of at most 0.015.
The roundings to bfloat16 on the way count: a program that leaves them out, or rounds other values in their place, can miss the bound.
Values may be sent and summed in bfloat16 or wider, within the bound.
A program may use at most 64 MiB of HBM per device.

v0:
```python
import jax
import jax.numpy as jnp
from jax import lax
from jax.sharding import PartitionSpec as P

EPG = 2


EPS = 1e-06


def over_pieces(value, axis):
    blocks = lax.all_gather(value, axis).astype(jnp.float32)
    return blocks.sum(axis=0)


def cut_along(value, dim, count):
    before, after = (value.shape[:dim], value.shape[dim + 1 :])
    return jnp.moveaxis(value.reshape(*before, count, -1, *after), dim, 0)


def sent_and_summed(value, axis, dim):
    count = lax.axis_size(axis)
    blocks = lax.all_to_all(cut_along(value, dim, count), axis, 0, 0, tiled=True)
    return jnp.sum(blocks.astype(jnp.float32), axis=0)


def rms_scale(values, gain):
    return values * lax.rsqrt(jnp.mean(values * values, axis=-1, keepdims=True) + EPS) * gain


def on_device(
    tokens,
    attn_gain,
    w_query,
    w_key,
    w_value,
    mix_lambda,
    head_gain,
    w_output,
    cache_keys,
    cache_value,
    lengths,
    moe_gain,
    group_ids,
    member_ids,
    group_gate,
    member_logits,
    w_exp_gate,
    w_exp_up,
    w_exp_down,
):
    seqs, width = tokens.shape
    resid_in = tokens.astype(jnp.float32)
    normed = rms_scale(resid_in, attn_gain).astype(jnp.bfloat16)
    heads_local = mix_lambda.shape[0]
    qk_cols = w_query.shape[1]
    head_dim = qk_cols // (2 * heads_local)
    stacked = jnp.concatenate([w_query, w_key, w_value], axis=1)
    projected = jnp.dot(
        normed,
        lax.all_gather(stacked, "ep", axis=0, tiled=True),
        preferred_element_type=jnp.float32,
    )
    projected = projected.astype(jnp.bfloat16)
    query = projected[:, :qk_cols]
    fresh_keys = projected[:, qk_cols : 2 * qk_cols]
    fresh_value = projected[:, 2 * qk_cols :]
    positions_all = cache_keys.shape[1]
    total_heads = heads_local * lax.axis_size("tp")
    head_index = (lax.axis_index("tp") * heads_local + jnp.arange(heads_local)).astype(jnp.float32)
    slopes = 2.0 ** (-8.0 * (head_index + 1.0) / total_heads)
    scale = head_dim ** (-0.5)
    positions = jnp.arange(positions_all)
    dist = (lengths[:, None] - positions[None, :]).astype(jnp.float32)
    valid = positions[None, :] < lengths[:, None]
    query4 = query.reshape(seqs, heads_local, 2, head_dim)
    keys5 = cache_keys.reshape(seqs, positions_all, heads_local, 2, head_dim)
    old = jnp.einsum("shcd,slhcd->cshl", query4, keys5, preferred_element_type=jnp.float32) * scale
    old = old - slopes[None, None, :, None] * dist[None, :, None, :]
    old = jnp.where(valid[None, :, None, :], old, -jnp.inf)
    fresh4 = fresh_keys.reshape(seqs, heads_local, 2, head_dim).astype(jnp.float32)
    new = jnp.moveaxis(jnp.sum(query4.astype(jnp.float32) * fresh4, axis=-1) * scale, 2, 0)
    full = jnp.concatenate([old, new[..., None]], axis=-1)
    maps = jax.nn.softmax(full, axis=-1)
    weights = (maps[0] - mix_lambda[None, :, None] * maps[1]).astype(jnp.bfloat16)
    values = cache_value.reshape(seqs, positions_all, heads_local, 2 * head_dim)
    head_mix = jnp.einsum(
        "shl,slhe->she", weights[..., :positions_all], values, preferred_element_type=jnp.float32
    )
    head_mix = head_mix + weights[..., positions_all].astype(jnp.float32)[
        ..., None
    ] * fresh_value.reshape(seqs, heads_local, 2 * head_dim).astype(jnp.float32)
    head_out = (
        rms_scale(head_mix, head_gain)
        .astype(jnp.bfloat16)
        .reshape(seqs, heads_local * 2 * head_dim)
    )
    term = jnp.dot(head_out, w_output, preferred_element_type=jnp.float32).astype(jnp.bfloat16)
    attn_sum = over_pieces(
        lax.optimization_barrier(term).astype(jnp.float32).astype(jnp.bfloat16), "tp"
    ).astype(jnp.float32)
    resid = resid_in + attn_sum
    moe_in = rms_scale(resid, moe_gain).astype(jnp.bfloat16)
    top = member_ids.shape[1]
    experts_local = w_exp_gate.shape[0]
    ep_count = lax.axis_size("ep")
    experts_all = experts_local * ep_count
    capacity = seqs * top // experts_all
    expert_ids = group_ids[:, None] * EPG + member_ids
    route_weight = jax.nn.softmax(member_logits, axis=-1) * group_gate[:, None]
    flat_ids = expert_ids.reshape(seqs * top)
    onehot = (flat_ids[:, None] == jnp.arange(experts_all)[None, :]).astype(jnp.int32)
    ranks = jnp.sum(jnp.cumsum(onehot, axis=0) * onehot, axis=1) - 1
    slot_grid = (flat_ids * capacity + ranks).reshape(seqs, top)
    slot_range = jnp.arange(experts_all * capacity)
    picker = jnp.sum((slot_grid[None, :, :] == slot_range[:, None, None]).astype(jnp.int32), axis=2)
    dispatch = jnp.dot(
        picker.astype(jnp.bfloat16), moe_in, preferred_element_type=jnp.float32
    ).astype(jnp.bfloat16)
    dispatch = dispatch.reshape(ep_count, experts_local, capacity, width)
    received = lax.all_to_all(dispatch, "ep", split_axis=0, concat_axis=2, tiled=True)
    received = received.reshape(experts_local, ep_count * capacity, width)
    gate = jnp.einsum("erd,edf->erf", received, w_exp_gate, preferred_element_type=jnp.float32)
    upper = jnp.einsum("erd,edf->erf", received, w_exp_up, preferred_element_type=jnp.float32)
    hidden = (jax.nn.silu(gate) * upper).astype(jnp.bfloat16)
    down = jnp.einsum("erf,efd->erd", hidden, w_exp_down, preferred_element_type=jnp.float32)
    summed = sent_and_summed(down.astype(jnp.bfloat16), "tp", 2).astype(jnp.bfloat16)
    cols = summed.shape[2]
    returned = lax.all_to_all(
        summed.reshape(experts_local, ep_count, capacity, cols),
        "ep",
        split_axis=1,
        concat_axis=0,
        tiled=True,
    )
    returned = returned.reshape(experts_all * capacity, cols)
    picked = returned[slot_grid].astype(jnp.float32)
    routed = jnp.sum(picked * route_weight[:, :, None], axis=1)
    own = lax.dynamic_slice_in_dim(resid, lax.axis_index("tp") * cols, cols, 1)
    mixed = (own + routed).astype(jnp.bfloat16)
    return (mixed, fresh_keys, fresh_value)


def solution(mesh):
    return jax.shard_map(
        on_device,
        mesh=mesh,
        in_specs=(
            P("ep", None),
            P(),
            P("ep", "tp"),
            P("ep", "tp"),
            P("ep", "tp"),
            P("tp"),
            P(),
            P("tp", None),
            P("ep", None, "tp"),
            P("ep", None, "tp"),
            P("ep"),
            P(),
            P("ep"),
            P("ep", None),
            P("ep"),
            P("ep", None),
            P("ep", None, "tp"),
            P("ep", None, "tp"),
            P("ep", "tp", None),
        ),
        out_specs=(P("ep", "tp"), P("ep", "tp"), P("ep", "tp")),
        check_vma=False,
    )
```

profile of v0, /device:TPU:8, one launch (start us, length us, event | category | flops | bytes accessed | tf_op | source)
XLA Modules:
  0.0 171.3 jit_solution(14302386364138983076)
XLA Ops:
  7.2 1.7 pad_maximum_fusion
  9.0 6.5 %copy.51 = bf16[16,1024,128]{1,2,0:T(8,128)(2,1)} copy(bf16[16,1024,128]{2,1,0:T(8,128)(2,1)} %param.27) | data formatting | bytes 8388608 | tf_op args[8]
  16.5 48.6 %all-gather.4.cloned.1.call-done = bf16[4096,384]{1,0:T(8,128)(2,1)} async-done(((bf16[256,384]{1,0:T(8,128)(2,1)}), bf16[4096,384]{1,0:T(8,128)(2,1)}) %all-gather.4.cloned.1.call-update) | async-done | bytes 3145744 | tf_op jit(solution)/shard_map/all_gather | solution.py:62
  65.1 2.4 %convolution_convert_fusion.3 = bf16[16,384]{1,0:T(8,128)(2,1)S(1)} fusion(bf16[4096,384]{1,0:T(8,128)(2,1)} %all-gather.4.cloned.1.call-done, bf16[16,4096]{1,0:T(8,128)(2,1)S(1)} %copy-done.1, f32[4096]{0:T(1024)S(1)} %copy-done.4, f32[16]{0:T(128)S(1)} %add_rsqrt_fusion.2), kind=kOutput, calls=%fused_computation.7 | convolution fusion | flops 50599936 | bytes 3305536 | tf_op jit(solution)/shard_map/dot_general | solution.py:60
  67.6 0.6 convert_multiply_fusion.3
  68.5 2.9 %fusion = f32[2,16,1,1024]{3,2,1,0:T(1,128)S(1)} fusion(bf16[16,1024,2,64]{1,3,2,0:T(8,128)(2,1)} %bitcast.56, bf16[16,2,64,1]{2,1,0,3:T(2,128)(2,1)S(1)} %reshape.379), kind=kOutput, calls=%fused_computation.5 | convolution fusion | flops 4194304 | bytes 4329472 | tf_op jit(solution)/shard_map/shcd,slhcd->cshl/dot_general | solution.py:79
  71.7 0.2 fusion.20
  72.1 2.8 %fusion.25 = f32[16,1,128]{2,1,0:T(1,128)S(1)} fusion(bf16[16,1024,128]{2,1,0:T(8,128)(2,1)} %param.28, bf16[16,1024,1]{1,0,2:T(8,128)(2,1)S(1)} %slice_bitcast_fusion), kind=kOutput, calls=%fused_computation.40 | convolution fusion | flops 4194304 | bytes 4235264 | tf_op jit(solution)/shard_map/shl,slhe->she/dot_general | solution.py:88
  75.0 0.2 multiply_reduce_fusion.2
  75.2 1.0 convolution_convert_fusion.2
  77.1 38.5 %all-gather.6.cloned.1.call-done = bf16[256,4096]{1,0:T(8,128)(2,1)} async-done(((bf16[16,4096]{1,0:T(8,128)(2,1)}), bf16[256,4096]{1,0:T(8,128)(2,1)}) %all-gather.6.cloned.1.call-update) | async-done | bytes 2097168 | tf_op jit(solution)/shard_map/all_gather | solution.py:13
  115.6 1.9 %convert_reduce_fusion = f32[16,4096]{1,0:T(8,128)S(1)} fusion(bf16[16,16,4096]{2,1,0:T(8,128)(2,1)} %bitcast.57), kind=kLoop, calls=%fused_computation.4 | loop fusion | flops 2031616 | bytes 2359296 | tf_op jit(solution)/shard_map/reduce_sum | solution.py:14
  117.8 0.3 convolution_convert_fusion.1
  118.2 14.2 %all_to_all.23 = bf16[16,1,2,4096]{3,2,1,0:T(2,128)(2,1)S(1)} all-to-all(bf16[16,1,2,4096]{3,2,1,0:T(2,128)(2,1)S(1)} %bitcast.59), channel_id=1, replica_groups=mesh['ep'=16,'tp'=16] {'ep'}, dimensions={0} | all-to-all | bytes 524288 | tf_op jit(solution)/shard_map/all_to_all | solution.py:122
  132.6 0.3 fusion.6
  132.9 1.8 %convolution_convert_fusion = bf16[32,4096]{1,0:T(8,128)(2,1)S(1)} fusion(bf16[32,4096]{1,0:T(8,128)(2,1)S(1)} %reshape.358, bf16[1,128,4096]{2,1,0:T(8,128)(2,1)S(1)} %copy-done, bf16[1,4096,128]{2,1,0:T(8,128)(2,1)} %param.36, f32[32,128]{1,0:T(8,128)S(1)} %fusion.6), kind=kOutput, calls=%fused_computation.1 | convolution fusion | flops 67264512 | bytes 2637824 | tf_op jit(solution)/shard_map/erf,efd->erd/dot_general | solution.py:127
  134.7 0.8 copy.78
  135.5 4.3 %all-to-all-start.1 = ((bf16[16,1,32,256]{3,2,1,0:T(8,128)(2,1)}), bf16[16,1,32,256]{3,2,1,0:T(8,128)(2,1)S(1)}, u32[]{:S(2)}, u32[]{:S(2)}) async-start(bf16[16,1,32,256]{3,2,1,0:T(8,128)(2,1)} %bitcast.54), calls=%async_computation.1 | async-start | bytes 524288 | tf_op jit(solution)/shard_map/all_to_all | solution.py:24
  139.9 11.0 %all-to-all-done.1 = bf16[16,1,32,256]{3,2,1,0:T(8,128)(2,1)S(1)} async-done(((bf16[16,1,32,256]{3,2,1,0:T(8,128)(2,1)}), bf16[16,1,32,256]{3,2,1,0:T(8,128)(2,1)S(1)}, u32[]{:S(2)}, u32[]{:S(2)}) %all-to-all-start.1) | async-done | bytes 262176 | tf_op jit(solution)/shard_map/all_to_all | solution.py:24
  150.9 0.6 reshape.363
  151.5 5.3 %all-to-all-start.2 = ((bf16[1,16,2,256]{3,2,0,1:T(2,128)(2,1)}), bf16[1,16,2,256]{3,2,0,1:T(2,128)(2,1)S(1)}, u32[]{:S(2)}, u32[]{:S(2)}) async-start(bf16[1,16,2,256]{3,2,0,1:T(2,128)(2,1)} %reshape.363), calls=%async_computation.2 | async-start | bytes 32768 | tf_op jit(solution)/shard_map/all_to_all | solution.py:130
  156.9 6.2 %all-to-all-done.2 = bf16[1,16,2,256]{3,2,0,1:T(2,128)(2,1)S(1)} async-done(((bf16[1,16,2,256]{3,2,0,1:T(2,128)(2,1)}), bf16[1,16,2,256]{3,2,0,1:T(2,128)(2,1)S(1)}, u32[]{:S(2)}, u32[]{:S(2)}) %all-to-all-start.2) | async-done | bytes 16416 | tf_op jit(solution)/shard_map/all_to_all | solution.py:130
  163.1 0.6 gather_fusion
  163.9 0.6 add_convert_fusion
  (75 shorter events, 3.1 us)
Async XLA Ops:
  7.2 125.7 %copy-start = (bf16[1,128,4096]{2,1,0:T(8,128)(2,1)S(1)}, bf16[1,128,4096]{2,1,0:T(8,128)(2,1)}, u32[]{:S(2)}) copy-start(bf16[1,128,4096]{2,1,0:T(8,128)(2,1)} %param.37) | copy-start | bytes 3145732
  7.2 57.9 %all-gather.4.cloned.1.call-start = ((), (), s32[]{:S(2)}) async-start(), calls=%async_computation.3 | async-start | bytes 3342336 | tf_op jit(solution)/shard_map/all_gather | solution.py:62
  8.9 106.7 %all-gather.6.cloned.1.call-start = ((), (), s32[]{:S(2)}) async-start(), calls=%async_computation.4 | async-start | bytes 2228224 | tf_op jit(solution)/shard_map/all_gather | solution.py:13
  9.0 7.2 %copy-start.1 = (bf16[16,4096]{1,0:T(8,128)(2,1)S(1)}, bf16[16,4096]{1,0:T(8,128)(2,1)}, u32[]{:S(2)}) copy-start(bf16[16,4096]{1,0:T(8,128)(2,1)} %param.19) | copy-start | bytes 393220
  9.0 7.3 %copy-start.8 = (s32[16]{0:T(128)S(1)}, s32[16]{0:T(128)}, u32[]{:S(2)}) copy-start(s32[16]{0:T(128)} %param.29) | copy-start | bytes 196
  9.0 56.1 %copy-start.4 = (f32[4096]{0:T(1024)S(1)}, f32[4096]{0:T(1024)}, u32[]{:S(2)}) copy-start(f32[4096]{0:T(1024)} %param.20) | copy-start | bytes 49156
  68.5 6.7 %copy-start.2 = (bf16[128,4096]{1,0:T(8,128)(2,1)S(1)}, bf16[128,4096]{1,0:T(8,128)(2,1)}, u32[]{:S(2)}) copy-start(bf16[128,4096]{1,0:T(8,128)(2,1)} %param.26) | copy-start | bytes 3145732
  68.5 6.7 %copy-start.10 = (f32[128]{0:T(128)S(1)}, f32[128]{0:T(128)}, u32[]{:S(2)}) copy-start(f32[128]{0:T(128)} %param.25) | copy-start | bytes 1540
  71.5 4.7 %copy-start.9 = (s32[16,2]{0,1:T(2,128)S(1)}, s32[16,2]{0,1:T(2,128)}, u32[]{:S(2)}) copy-start(s32[16,2]{0,1:T(2,128)} %param.32) | copy-start | bytes 388
  71.5 4.8 %copy-start.12 = (s32[16]{0:T(128)S(1)}, s32[16]{0:T(128)}, u32[]{:S(2)}) copy-start(s32[16]{0:T(128)} %param.31) | copy-start | bytes 196
  72.1 45.6 %copy-start.6 = (f32[4096]{0:T(1024)S(1)}, f32[4096]{0:T(1024)}, u32[]{:S(2)}) copy-start(f32[4096]{0:T(1024)} %param.30) | copy-start | bytes 49156
  75.0 57.6 %copy-start.3 = (bf16[1,4096,128]{2,1,0:T(8,128)(2,1)S(1)}, bf16[1,4096,128]{2,1,0:T(8,128)(2,1)}, u32[]{:S(2)}) copy-start(bf16[1,4096,128]{2,1,0:T(8,128)(2,1)} %param.35) | copy-start | bytes 3145732
  75.2 59.4 %copy-start.5 = (bf16[16,128]{1,0:T(8,128)(2,1)}, bf16[16,128]{1,0:T(8,128)(2,1)S(1)}, u32[]{:S(2)}) copy-start(bf16[16,128]{1,0:T(8,128)(2,1)S(1)} %get-tuple-element.8) | copy-start | bytes 12292
  117.5 22.3 %copy-start.7 = (f32[16,2]{0,1:T(2,128)S(1)}, f32[16,2]{0,1:T(2,128)}, u32[]{:S(2)}) copy-start(f32[16,2]{0,1:T(2,128)} %param.34) | copy-start | bytes 388
  117.6 22.3 %copy-start.11 = (f32[16]{0:T(128)S(1)}, f32[16]{0:T(128)}, u32[]{:S(2)}) copy-start(f32[16]{0:T(128)} %param.33) | copy-start | bytes 196
  135.5 15.4 %all-to-all-start.1 = ((bf16[16,1,32,256]{3,2,1,0:T(8,128)(2,1)}), bf16[16,1,32,256]{3,2,1,0:T(8,128)(2,1)S(1)}, u32[]{:S(2)}, u32[]{:S(2)}) async-start(bf16[16,1,32,256]{3,2,1,0:T(8,128)(2,1)} %bitcast.54), calls=%async_computation.1 | async-start | bytes 524288 | tf_op jit(solution)/shard_map/all_to_all | solution.py:24
  151.5 11.6 %all-to-all-start.2 = ((bf16[1,16,2,256]{3,2,0,1:T(2,128)(2,1)}), bf16[1,16,2,256]{3,2,0,1:T(2,128)(2,1)S(1)}, u32[]{:S(2)}, u32[]{:S(2)}) async-start(bf16[1,16,2,256]{3,2,0,1:T(2,128)(2,1)} %reshape.363), calls=%async_computation.2 | async-start | bytes 32768 | tf_op jit(solution)/shard_map/all_to_all | solution.py:130
Sparse Core Ops, SparseCore 0:
  10.4 54.6 all-gather.3
  76.3 39.2 all-gather.5
where the time goes:
time: 174 us; the launch traced here: 171 us
  waiting for transfers between devices  104 us (60%)
  between operations  15 us (9%)
  blocking collectives  14.2 us (8%)
  matrix products  11.5 us (7%)
  local copies, waits for them, and re-layouts  9.73 us (6%)
  starting transfers between devices  9.62 us (6%)
  other arithmetic  6.9 us (4%)
    all_gather x1, waiting for transfers between devices, on_device(): lax.all_gather(stacked, 'ep', axis=0, tiled=True)  48.6 us
    all_gather x1, waiting for transfers between devices, over_pieces(): blocks = lax.all_gather(value, axis).astype(jnp.float32)  38.5 us
    all_to_all x1, blocking collectives, on_device(): lax.all_to_all(dispatch, 'ep', split_axis=0, concat_axis=2, tiled=True)  14.2 us
    all_to_all x1, waiting for transfers between devices, sent_and_summed(): lax.all_to_all(cut_along(value, dim, count), axis, 0, 0, tiled=True)  11 us
    unnamed x30, local copies, waits for them, and re-layouts  6.74 us
    all_to_all x1, waiting for transfers between devices, on_device(): lax.all_to_all(summed.reshape(experts_local, ep_count, capacity, cols), '...  6.2 us
    all_to_all x1, starting transfers between devices, on_device(): lax.all_to_all(summed.reshape(experts_local, ep_count, capacity, cols), '...  5.29 us
    all_to_all x1, starting transfers between devices, sent_and_summed(): lax.all_to_all(cut_along(value, dim, count), axis, 0, 0, tiled=True)  4.25 us
  transfers between devices with their start and end apart: 4, of which 4 were waited for; matrix products, arithmetic and copies ran while one was open for 5% of the time, Pallas kernels for 0%

commit v1 on v0

v1 whole, which is shorter than its diff:
```python
import functools

import jax
import jax.numpy as jnp
from jax import lax
from jax.experimental import pallas as pl
from jax.experimental.pallas import tpu as pltpu
from jax.sharding import PartitionSpec as P

EPG = 2
EPS = 1e-06
MESH = pl.DeviceIdType.MESH
HIGHEST = lax.Precision.HIGHEST
F32 = jnp.float32
BF16 = jnp.bfloat16
NT = (((1,), (1,)), ((), ()))


def iota(shape, dim):
    return lax.broadcasted_iota(jnp.int32, shape, dim)


def exact_dot(a, b, dims=(((1,), (0,)), ((), ()))):
    return lax.dot_general(a, b, dims, precision=HIGHEST, preferred_element_type=F32)


def layer_kernel(
    n,
    tokens_h,
    attn_gain_h,
    wq_h,
    wk_h,
    wv_h,
    lam_ref,
    head_gain_h,
    wo_h,
    keys_h,
    vals_h,
    lengths_ref,
    moe_gain_h,
    groups_ref,
    members_ref,
    gates_ref,
    logits_ref,
    wg_h,
    wu_h,
    wd_h,
    mixed_ref,
    fresh_k_ref,
    fresh_v_ref,
    tokens,
    attn_gain,
    wqkv,
    head_gain,
    wo,
    keys,
    vals,
    moe_gain,
    wgu,
    wd,
    rows_s,
    send_a,
    recv_a,
    send_b,
    recv_b,
    send_c,
    recv_c,
    send_e,
    recv_e,
    send_f,
    recv_f,
    send_s,
    recv_s,
    send_g,
    recv_g,
    send_h,
    recv_h,
    load_sem,
    ss,
    rs,
):
    ep = lax.axis_index("ep")
    tp = lax.axis_index("tp")
    width = tokens_h.shape[1]
    cols = width // n
    seqs = tokens_h.shape[0]
    hd = wq_h.shape[1]
    half = hd // 2
    cache = keys_h.shape[1]

    loads = [
        (tokens_h, tokens),
        (attn_gain_h, attn_gain),
        (wq_h, wqkv.at[:, pl.ds(0, hd)]),
        (wk_h, wqkv.at[:, pl.ds(hd, hd)]),
        (wv_h, wqkv.at[:, pl.ds(2 * hd, hd)]),
        (keys_h, keys),
        (vals_h, vals),
        (head_gain_h, head_gain),
        (wo_h, wo),
        (moe_gain_h, moe_gain),
        (wg_h.at[0], wgu.at[:, pl.ds(0, hd)]),
        (wu_h.at[0], wgu.at[:, pl.ds(hd, hd)]),
        (wd_h.at[0], wd),
    ]
    copies = [pltpu.make_async_copy(s, d, load_sem.at[i]) for i, (s, d) in enumerate(loads)]
    for copy in copies:
        copy.start()

    barrier = pltpu.get_barrier_semaphore()

    def greet(d, carry):
        pl.semaphore_signal(barrier, inc=1, device_id=(lax.rem(ep + d, n), tp), device_id_type=MESH)
        pl.semaphore_signal(barrier, inc=1, device_id=(ep, lax.rem(tp + d, n)), device_id_type=MESH)
        return carry

    lax.fori_loop(1, n, greet, 0)

    def block(ref, i, tiles):
        return ref.at[pl.ds(pl.multiple_of(i * 8, 8), 8), :] if tiles else ref.at[i]

    def exchange(phase, send, recv, over_ep, whole=False, tiles=False):
        me = ep if over_ep else tp

        def descriptor(d, incoming):
            peer = lax.rem(me + d, n)
            slot = peer if incoming else me
            target = (peer, tp) if over_ep else (ep, peer)
            return pltpu.make_async_remote_copy(
                src_ref=send if whole else block(send, peer, tiles),
                dst_ref=block(recv, slot, tiles),
                send_sem=ss.at[phase, peer],
                recv_sem=rs.at[phase, slot],
                device_id=target,
                device_id_type=MESH,
            )

        def start(d, carry):
            descriptor(d, False).start()
            return carry

        def arrived(d):
            descriptor(d, True).wait_recv()

        def sent(d, carry):
            descriptor(d, False).wait_send()
            return carry

        return start, arrived, sent

    def wait_all(arrived):
        def body(d, carry):
            arrived(d)
            return carry

        lax.fori_loop(1, n, body, 0)

    a_start, a_arrived, a_sent = exchange(0, send_a, recv_a, True)
    b_start, b_arrived, b_sent = exchange(1, send_b, recv_b, True)
    c_start, c_arrived, c_sent = exchange(2, send_c, recv_c, False)
    e_start, e_arrived, e_sent = exchange(3, send_e, recv_e, True, tiles=True)
    f_start, f_arrived, f_sent = exchange(4, send_f, recv_f, False, True)
    s_start, s_arrived, s_sent = exchange(5, send_s, recv_s, False, True)
    g_start, g_arrived, g_sent = exchange(6, send_g, recv_g, False)
    h_start, h_arrived, h_sent = exchange(7, send_h, recv_h, True, tiles=True)

    copies[0].wait()
    copies[1].wait()
    x = tokens[...].astype(F32)
    normed = x * lax.rsqrt(jnp.mean(x * x, axis=-1, keepdims=True) + EPS) * attn_gain[...]
    normed = normed.astype(BF16)
    for i in range(n):
        send_a[i] = normed[:, i * cols : (i + 1) * cols]
    recv_a[ep] = send_a[ep]
    pl.semaphore_wait(barrier, 2 * (n - 1))
    lax.fori_loop(1, n, a_start, 0)

    rows_s[...] = jnp.zeros_like(rows_s)
    rows_s[0:1, 0:seqs] = lengths_ref[...].astype(F32)
    rows_s[1:2, 0:seqs] = groups_ref[...].astype(F32)
    rows_s[2:4, 0:seqs] = members_ref[...].astype(F32)
    rows_s[4:5, 0:seqs] = gates_ref[...]
    rows_s[5:7, 0:seqs] = logits_ref[...]
    rows = rows_s[...][:, 0:seqs]
    eye = (iota((seqs, seqs), 0) == iota((seqs, seqs), 1)).astype(F32)
    columns = exact_dot(eye, rows, NT)
    id0_row = rows[1:2] * EPG + rows[2:3]
    id1_row = rows[1:2] * EPG + rows[3:4]
    id0_col = columns[:, 1:2] * EPG + columns[:, 2:3]
    id1_col = columns[:, 1:2] * EPG + columns[:, 3:4]
    logit_max = jnp.maximum(columns[:, 5:6], columns[:, 6:7])
    exp0 = jnp.exp(columns[:, 5:6] - logit_max)
    exp1 = jnp.exp(columns[:, 6:7] - logit_max)
    exp_sum = exp0 + exp1
    share0 = exp0 / exp_sum * columns[:, 4:5]
    share1 = exp1 / exp_sum * columns[:, 4:5]
    tall = 8 * n
    tall_row = iota((tall, seqs), 0)
    tall_expert = (tall_row // 8).astype(F32)
    tall_kind = tall_row % 8
    tall_rank = jnp.where((tall_kind == 2) | (tall_kind == 3) | (tall_kind == 5), 1.0, 0.0)
    chosen = ((id0_row == tall_expert) | (id1_row == tall_expert)).astype(F32)
    before = (iota((seqs, seqs), 0) < iota((seqs, seqs), 1)).astype(F32)
    rank = exact_dot(chosen, before)
    dispatch = jnp.where((rank == tall_rank) & (tall_kind < 6), chosen, 0.0)
    wide_col = iota((seqs, tall), 1)
    wide_expert = (wide_col // 8).astype(F32)
    wide_kind = wide_col % 8
    wide_rank = jnp.where(wide_kind >= 2, 1.0, 0.0)
    hit0 = (id0_col == wide_expert).astype(F32)
    hit1 = (id1_col == wide_expert).astype(F32)
    after = (iota((seqs, seqs), 1) < iota((seqs, seqs), 0)).astype(F32)
    wide_ranks = exact_dot(after, hit0 + hit1)
    combine = jnp.where((wide_ranks == wide_rank) & (wide_kind < 4), hit0 * share0 + hit1 * share1, 0.0)

    wait_all(a_arrived)
    for i in (2, 3, 4):
        copies[i].wait()
    everyone = recv_a[...].reshape(n * seqs, cols)
    partial = jnp.dot(everyone, wqkv[...], preferred_element_type=F32)
    send_b[...] = partial.reshape(n, seqs, 3 * hd)
    recv_b[ep] = send_b[ep]
    lax.fori_loop(1, n, b_start, 0)
    wait_all(b_arrived)
    projected = jnp.sum(recv_b[...], axis=0).astype(BF16)
    query = projected[:, 0:hd]
    fresh_k = projected[:, hd : 2 * hd]
    fresh_v = projected[:, 2 * hd : 3 * hd]
    fresh_k_ref[...] = fresh_k
    fresh_v_ref[...] = fresh_v

    total_heads = n
    slope = jnp.float32(0.0)
    for h in range(total_heads):
        slope = jnp.where(tp == h, jnp.float32(2.0 ** (-8.0 * (h + 1.0) / total_heads)), slope)
    scale = half ** (-0.5)
    both = 2 * seqs
    q2 = jnp.concatenate([query, query], axis=0).astype(F32)
    k2 = jnp.concatenate([fresh_k, fresh_k], axis=0).astype(F32)
    own_map = (iota((both, hd), 0) // seqs) == (iota((both, hd), 1) // half)
    q2 = jnp.where(own_map, q2, 0.0)
    new = jnp.sum(q2 * k2, axis=-1, keepdims=True) * scale
    q4 = jnp.concatenate([q2, q2], axis=1)
    q4_seq = iota((both, 2 * hd), 0) % seqs
    q4_side = iota((both, 2 * hd), 1) // hd
    copies[5].wait()

    def score_step(p, acc):
        lhs = jnp.where(q4_seq == 2 * p + q4_side, q4, 0.0).astype(BF16)
        rhs = jnp.concatenate([keys[2 * p], keys[2 * p + 1]], axis=1)
        return acc + lax.dot_general(lhs, rhs, NT, preferred_element_type=F32)

    old = lax.fori_loop(0, seqs // 2, score_step, jnp.zeros((both, cache), F32)) * scale
    count = jnp.concatenate([columns[:, 0:1], columns[:, 0:1]], axis=0)
    place = iota((both, cache), 1).astype(F32)
    old = jnp.where(place < count, old - slope * (count - place), -jnp.inf)
    top = jnp.maximum(jnp.max(old, axis=-1, keepdims=True), new)
    e_old = jnp.exp(old - top)
    e_new = jnp.exp(new - top)
    norm = jnp.sum(e_old, axis=-1, keepdims=True) + e_new
    m_old = e_old / norm
    m_new = e_new / norm
    lam = lam_ref[...]
    weights = (m_old[:seqs] - lam * m_old[seqs:]).astype(BF16).astype(F32)
    w_new = (m_new[:seqs] - lam * m_new[seqs:]).astype(BF16).astype(F32)
    w_pair = iota((seqs, cache), 0) // 2
    copies[6].wait()

    def value_step(p, acc):
        lhs = jnp.where(w_pair == p, weights, 0.0).astype(BF16)
        rhs = jnp.concatenate([vals[2 * p], vals[2 * p + 1]], axis=1)
        return acc + jnp.dot(lhs, rhs, preferred_element_type=F32)

    mix = lax.fori_loop(0, seqs // 2, value_step, jnp.zeros((seqs, 2 * hd), F32))
    head_mix = jnp.where(iota((seqs, hd), 0) % 2 == 0, mix[:, :hd], mix[:, hd:])
    head_mix = head_mix + w_new * fresh_v.astype(F32)
    copies[7].wait()
    head_out = head_mix * lax.rsqrt(jnp.mean(head_mix * head_mix, axis=-1, keepdims=True) + EPS)
    head_out = (head_out * head_gain[...]).astype(BF16)

    copies[8].wait()
    for i in range(n):
        term = jnp.dot(head_out, wo[:, i * cols : (i + 1) * cols], preferred_element_type=F32)
        send_c[i] = term.astype(BF16)
    recv_c[tp] = send_c[tp]
    lax.fori_loop(1, n, c_start, 0)
    wait_all(c_arrived)
    attn_sum = jnp.sum(recv_c[...].astype(F32), axis=0)
    own_cols = pl.ds(pl.multiple_of(tp * cols, cols), cols)
    resid = tokens[:, own_cols].astype(F32) + attn_sum

    squares = jnp.broadcast_to(jnp.sum(resid * resid, axis=-1, keepdims=True), (seqs, 128))
    first = (tall_kind == 0) | (tall_kind == 2)
    second = (tall_kind == 1) | (tall_kind == 3)
    packed = exact_dot(jnp.where(first, dispatch, 0.0), resid[:, :128])
    packed += exact_dot(jnp.where(second, dispatch, 0.0), resid[:, 128:])
    packed += exact_dot(jnp.where(tall_kind >= 4, dispatch, 0.0), squares)
    send_e[...] = packed
    recv_e[pl.ds(pl.multiple_of(ep * 8, 8), 8), :] = send_e[pl.ds(pl.multiple_of(ep * 8, 8), 8), :]

    lax.fori_loop(1, n, e_start, 0)
    wait_all(e_arrived)

    def tile_row(ref, j):
        return ref[pl.ds(j, n, stride=8), :]

    token_rows = [
        jnp.concatenate([tile_row(recv_e, 2 * r), tile_row(recv_e, 2 * r + 1)], axis=1) for r in range(2)
    ]
    slab = jnp.concatenate(token_rows, axis=0)
    copies[9].wait()
    send_f[...] = (slab * moe_gain[:, own_cols]).astype(BF16)
    on_lane = iota((n, 128), 0) == iota((n, 128), 1)
    on_next = iota((n, 128), 0) + n == iota((n, 128), 1)
    stat = jnp.where(on_lane, tile_row(recv_e, 4), 0.0) + jnp.where(on_next, tile_row(recv_e, 5), 0.0)
    send_s[...] = jnp.broadcast_to(jnp.sum(stat, axis=0, keepdims=True), (8, 128))
    recv_f[tp] = send_f[...]
    recv_s[tp] = send_s[...]

    lax.fori_loop(1, n, s_start, 0)
    lax.fori_loop(1, n, f_start, 0)
    for i in (10, 11):
        copies[i].wait()
    slots = 2 * n

    def up_block(peer):
        at = pl.ds(pl.multiple_of(peer * cols, cols), cols)
        return jnp.dot(recv_f[peer], wgu[at, :], preferred_element_type=F32)

    def up_step(d, acc):
        f_arrived(d)
        return acc + up_block(lax.rem(tp + d, n))

    gate_up = lax.fori_loop(1, n, up_step, up_block(tp))
    wait_all(s_arrived)
    stats = jnp.sum(recv_s[...], axis=0)
    eye_slots = (iota((slots, 128), 0) == iota((slots, 128), 1)).astype(F32)
    sums = exact_dot(eye_slots, stats, NT)[:, 0:1]
    norm_scale = lax.rsqrt(sums / width + EPS)
    gate = gate_up[:, :hd] * norm_scale
    upper = gate_up[:, hd:] * norm_scale
    hidden = (gate / (1.0 + jnp.exp(-gate)) * upper).astype(BF16)

    copies[12].wait()
    for i in range(n):
        down = jnp.dot(hidden, wd[:, i * cols : (i + 1) * cols], preferred_element_type=F32)
        send_g[i] = down.astype(BF16)
    recv_g[tp] = send_g[tp]
    lax.fori_loop(1, n, g_start, 0)
    wait_all(g_arrived)
    expert_out = jnp.sum(recv_g[...].astype(F32), axis=0).astype(BF16).astype(F32)

    send_h[...] = jnp.zeros_like(send_h)
    for r in range(2):
        for h in range(2):
            send_h[pl.ds(2 * r + h, n, stride=8), :] = expert_out[r * n : (r + 1) * n, h * 128 : (h + 1) * 128]
    recv_h[pl.ds(pl.multiple_of(ep * 8, 8), 8), :] = send_h[pl.ds(pl.multiple_of(ep * 8, 8), 8), :]
    lax.fori_loop(1, n, h_start, 0)
    wait_all(h_arrived)
    back = recv_h[...]
    routed = [exact_dot(jnp.where(wide_kind % 2 == h, combine, 0.0), back) for h in range(2)]
    mixed_ref[...] = (resid + jnp.concatenate(routed, axis=1)).astype(BF16)

    for sent in (a_sent, b_sent, c_sent, e_sent, f_sent, s_sent, g_sent, h_sent):
        lax.fori_loop(1, n, sent, 0)


def on_device(n, *args):
    (tokens, attn_gain, w_query, w_key, w_value, mix_lambda, head_gain, w_output, cache_keys, cache_value) = args[:10]
    (lengths, moe_gain, group_ids, member_ids, group_gate, member_logits, w_exp_gate, w_exp_up, w_exp_down) = args[10:]
    seqs, width = tokens.shape
    cols = width // n
    hd = w_query.shape[1]
    cache = cache_keys.shape[1]
    operands = (
        tokens,
        attn_gain.reshape(1, width),
        w_query,
        w_key,
        w_value,
        mix_lambda.reshape(1, 1),
        head_gain.reshape(1, hd),
        w_output,
        cache_keys,
        cache_value,
        lengths.reshape(1, seqs),
        moe_gain.reshape(1, width),
        group_ids.reshape(1, seqs),
        member_ids.T,
        group_gate.reshape(1, seqs),
        member_logits.T,
        w_exp_gate,
        w_exp_up,
        w_exp_down,
    )
    small = (5, 10, 12, 13, 14, 15)
    vmem = pl.BlockSpec(memory_space=pltpu.VMEM)
    hbm = pl.BlockSpec(memory_space=pl.ANY)
    scratch = [
        pltpu.VMEM((seqs, width), BF16),
        pltpu.VMEM((1, width), F32),
        pltpu.VMEM((w_query.shape[0], 3 * hd), BF16),
        pltpu.VMEM((1, hd), F32),
        pltpu.VMEM((hd, width), BF16),
        pltpu.VMEM((seqs, cache, hd), BF16),
        pltpu.VMEM((seqs, cache, hd), BF16),
        pltpu.VMEM((1, width), F32),
        pltpu.VMEM((width, 2 * hd), BF16),
        pltpu.VMEM((hd, width), BF16),
        pltpu.VMEM((8, 128), F32),
        pltpu.VMEM((n, seqs, cols), BF16),
        pltpu.VMEM((n, seqs, cols), BF16),
        pltpu.VMEM((n, seqs, 3 * hd), F32),
        pltpu.VMEM((n, seqs, 3 * hd), F32),
        pltpu.VMEM((n, seqs, cols), BF16),
        pltpu.VMEM((n, seqs, cols), BF16),
        pltpu.VMEM((8 * n, 128), F32),
        pltpu.VMEM((8 * n, 128), F32),
        pltpu.VMEM((2 * n, cols), BF16),
        pltpu.VMEM((n, 2 * n, cols), BF16),
        pltpu.VMEM((8, 128), F32),
        pltpu.VMEM((n, 8, 128), F32),
        pltpu.VMEM((n, 2 * n, cols), BF16),
        pltpu.VMEM((n, 2 * n, cols), BF16),
        pltpu.VMEM((8 * n, 128), F32),
        pltpu.VMEM((8 * n, 128), F32),
        pltpu.SemaphoreType.DMA((13,)),
        pltpu.SemaphoreType.DMA((8, n)),
        pltpu.SemaphoreType.DMA((8, n)),
    ]
    return pl.pallas_call(
        functools.partial(layer_kernel, n),
        out_shape=(
            jax.ShapeDtypeStruct((seqs, cols), BF16),
            jax.ShapeDtypeStruct((seqs, hd), BF16),
            jax.ShapeDtypeStruct((seqs, hd), BF16),
        ),
        in_specs=[vmem if i in small else hbm for i in range(len(operands))],
        out_specs=(vmem, vmem, vmem),
        scratch_shapes=scratch,
        compiler_params=pltpu.CompilerParams(collective_id=0, has_side_effects=True),
        name="layer",
    )(*operands)


def solution(mesh):
    n = mesh.shape["ep"]
    return jax.shard_map(
        functools.partial(on_device, n),
        mesh=mesh,
        in_specs=(
            P("ep", None),
            P(),
            P("ep", "tp"),
            P("ep", "tp"),
            P("ep", "tp"),
            P("tp"),
            P(),
            P("tp", None),
            P("ep", None, "tp"),
            P("ep", None, "tp"),
            P("ep"),
            P(),
            P("ep"),
            P("ep", None),
            P("ep"),
            P("ep", None),
            P("ep", None, "tp"),
            P("ep", None, "tp"),
            P("ep", "tp", None),
        ),
        out_specs=(P("ep", "tp"), P("ep", "tp"), P("ep", "tp")),
        check_vma=False,
    )
```

time: 174 us -> 71.5 us (0.41)
  waiting for transfers between devices: 104 us -> 0 us
  Pallas kernels: 0 us -> 65 us
  blocking collectives: 14.2 us -> 0 us
  between operations: 15 us -> 1.29 us
  matrix products: 11.5 us -> 0 us
  starting transfers between devices: 9.62 us -> 0 us
  other arithmetic: 6.9 us -> 0 us
  local copies, waits for them, and re-layouts: 9.73 us -> 3.83 us
    all_gather x2 -> x0, waiting for transfers between devices: 87.1 us -> none  [the longest x1 48.6 us: on_device(): lax.all_gather(stacked, 'ep', axis=0, tiled=True)]
    pallas_call x0 -> x1, Pallas kernels: none -> 65 us  [on_device(): pl.pallas_call(functools.partial(layer_kernel, n), out_shape=(jax.ShapeDt...]
    all_to_all x2 -> x0, waiting for transfers between devices: 17.2 us -> none  [the longest x1 11 us: sent_and_summed(): lax.all_to_all(cut_along(value, dim, count), axis, 0, 0, tiled=True)]
    all_to_all x1 -> x0, blocking collectives: 14.2 us -> none  [on_device(): lax.all_to_all(dispatch, 'ep', split_axis=0, concat_axis=2, tiled=True)]
    dot_general x7 -> x0, matrix products: 11.5 us -> none  [the longest x1 2.93 us: on_device(): jnp.einsum('shcd,slhcd->cshl', query4, keys5, preferred_element_type=jnp....]
    all_to_all x2 -> x0, starting transfers between devices: 9.54 us -> none  [the longest x1 5.29 us: on_device(): lax.all_to_all(summed.reshape(experts_local, ep_count, capacity, cols), '...]
    reduce_sum x11 -> x0, other arithmetic: 3.13 us -> none  [the longest x1 1.92 us: over_pieces(): return blocks.sum(axis=0)]
    unnamed x30 -> x3, local copies, waits for them, and re-layouts: 6.74 us -> 3.83 us
  transfers between devices with their start and end apart: 4 -> 0, of which waited for: 4 -> 0; matrix products, arithmetic and copies ran while one was open for 5% -> 0% of each run, Pallas kernels for 0% -> 0%
where the time goes in v1:
time: 71.5 us; the launch traced here: 70.1 us
  Pallas kernels  65 us (91%)
  local copies, waits for them, and re-layouts  3.83 us (5%)
  between operations  1.29 us (2%)
    pallas_call x1, Pallas kernels, on_device(): pl.pallas_call(functools.partial(layer_kernel, n), out_shape=(jax.ShapeDt...  65 us
    unnamed x3, local copies, waits for them, and re-layouts  3.83 us

profile of v1, /device:TPU:8, one launch (start us, length us, event | category | flops | bytes accessed | tf_op | source)
XLA Modules:
  0.0 70.1 jit_solution(2518249397619897832)
XLA Ops:
  1.3 65.0 %layer.1 = (bf16[16,256]{1,0:T(8,128)(2,1)}, bf16[16,128]{1,0:T(8,128)(2,1)}, bf16[16,128]{1,0:T(8,128)(2,1)}) custom-call(bf16[16,4096]{1,0:T(8,128)(2,1)} %tokens_h.1, f32[1,4096]{1,0:T(1,128)} %bitcast.10, bf16[256,128]{1,0:T(8,128)(2,1)} %wq_h.1, bf16[256,128]{1,0:T(8,128)(2,1)} %wk_h.1, bf16[256,128]{1,0:T(8,128)(2,1)} %wv_h.1, f32[1,1]{1,0:T(1,128)} %bitcast.9.lam_ref, ...), custom_call_target="tpu_custom_call" | custom-call | tf_op jit(solution)/shard_map/layer/pallas_call | solution.py:431
  66.3 1.3 %copy.26 = bf16[16,256]{1,0:T(8,128)(2,1)} copy(bf16[16,256]{1,0:T(8,128)(2,1)} %get-tuple-element.6) | data formatting | bytes 16384
  67.6 1.3 %copy.27 = bf16[16,128]{1,0:T(8,128)(2,1)} copy(bf16[16,128]{1,0:T(8,128)(2,1)} %get-tuple-element.7) | data formatting | bytes 8192
  68.8 1.3 %copy.28 = bf16[16,128]{1,0:T(8,128)(2,1)} copy(bf16[16,128]{1,0:T(8,128)(2,1)} %get-tuple-element.8) | data formatting | bytes 8192

commit v2 on v1

--- a/solution.py
+++ b/solution.py
@@ -31,26 +31,30 @@
     wq_h,
     wk_h,
     wv_h,
-    lam_ref,
+    lam_h,
     head_gain_h,
     wo_h,
     keys_h,
     vals_h,
+    lengths_h,
+    moe_gain_h,
+    groups_h,
+    members_h,
+    gates_h,
+    logits_h,
+    wg_h,
+    wu_h,
+    wd_h,
+    out_ref,
+    tokens,
+    attn_gain,
+    wqkv,
+    lam_ref,
     lengths_ref,
-    moe_gain_h,
     groups_ref,
     members_ref,
     gates_ref,
     logits_ref,
-    wg_h,
-    wu_h,
-    wd_h,
-    mixed_ref,
-    fresh_k_ref,
-    fresh_v_ref,
-    tokens,
-    attn_gain,
-    wqkv,
     head_gain,
     wo,
     keys,
@@ -71,6 +75,9 @@
     recv_f,
     send_s,
     recv_s,
+    pair_out,
+    pair_in,
+    pair_own,
     send_g,
     recv_g,
     send_h,
@@ -88,25 +95,6 @@
     half = hd // 2
     cache = keys_h.shape[1]
 
-    loads = [
-        (tokens_h, tokens),
-        (attn_gain_h, attn_gain),
-        (wq_h, wqkv.at[:, pl.ds(0, hd)]),
-        (wk_h, wqkv.at[:, pl.ds(hd, hd)]),
-        (wv_h, wqkv.at[:, pl.ds(2 * hd, hd)]),
-        (keys_h, keys),
-        (vals_h, vals),
-        (head_gain_h, head_gain),
-        (wo_h, wo),
-        (moe_gain_h, moe_gain),
-        (wg_h.at[0], wgu.at[:, pl.ds(0, hd)]),
-        (wu_h.at[0], wgu.at[:, pl.ds(hd, hd)]),
-        (wd_h.at[0], wd),
-    ]
-    copies = [pltpu.make_async_copy(s, d, load_sem.at[i]) for i, (s, d) in enumerate(loads)]
-    for copy in copies:
-        copy.start()
-
     barrier = pltpu.get_barrier_semaphore()
 
     def greet(d, carry):
@@ -116,14 +104,56 @@
 
     lax.fori_loop(1, n, greet, 0)
 
+    loads = {
+        "tokens": (tokens_h, tokens),
+        "attn_gain": (attn_gain_h, attn_gain),
+        "wq": (wq_h, wqkv.at[:, pl.ds(0, hd)]),
+        "wk": (wk_h, wqkv.at[:, pl.ds(hd, hd)]),
+        "wv": (wv_h, wqkv.at[:, pl.ds(2 * hd, hd)]),
+        "lengths": (lengths_h, lengths_ref),
+        "groups": (groups_h, groups_ref),
+        "members": (members_h, members_ref),
+        "gates": (gates_h, gates_ref),
+        "logits": (logits_h, logits_ref),
+        "head_gain": (head_gain_h, head_gain),
+        "moe_gain": (moe_gain_h, moe_gain),
+        "keys": (keys_h, keys),
+        "vals": (vals_h, vals),
+        "wo": (wo_h, wo),
+        "wg": (wg_h.at[0], wgu.at[:, pl.ds(0, hd)]),
+        "wu": (wu_h.at[0], wgu.at[:, pl.ds(hd, hd)]),
+        "wd": (wd_h.at[0], wd),
+    }
+    copies = {
+        name: pltpu.make_async_copy(source, target, load_sem.at[i])
+        for i, (name, (source, target)) in enumerate(loads.items())
+    }
+    late = ("keys", "vals", "wo", "wg", "wu", "wd")
+    for name, copy in copies.items():
+        if name not in late:
+            copy.start()
+
+    def far_first(over_ep):
+        if over_ep:
+            side = 4
+            offsets = [(a, b) for a in range(side) for b in range(n // side) if (a, b) != (0, 0)]
+            offsets.sort(key=lambda o: -(min(o[0], side - o[0]) + min(o[1], n // side - o[1])))
+            for a, b in offsets:
+                yield lax.rem(ep // side + a, side) * side + lax.rem(ep % side + b, side)
+        else:
+            chips = n // 2
+            offsets = [(a, b) for a in range(chips) for b in range(2) if (a, b) != (0, 0)]
+            offsets.sort(key=lambda o: -min(o[0], chips - o[0]))
+            for a, b in offsets:
+                yield lax.rem(tp // 2 + a, chips) * 2 + lax.rem(tp % 2 + b, 2)
+
     def block(ref, i, tiles):
         return ref.at[pl.ds(pl.multiple_of(i * 8, 8), 8), :] if tiles else ref.at[i]
 
     def exchange(phase, send, recv, over_ep, whole=False, tiles=False):
         me = ep if over_ep else tp
 
-        def descriptor(d, incoming):
-            peer = lax.rem(me + d, n)
+        def descriptor(peer, incoming):
             slot = peer if incoming else me
             target = (peer, tp) if over_ep else (ep, peer)
             return pltpu.make_async_remote_copy(
@@ -135,15 +165,15 @@
                 device_id_type=MESH,
             )
 
-        def start(d, carry):
-            descriptor(d, False).start()
-            return carry
+        def start():
+            for peer in far_first(over_ep):
+                descriptor(peer, False).start()
 
         def arrived(d):
-            descriptor(d, True).wait_recv()
+            descriptor(lax.rem(me + d, n), True).wait_recv()
 
         def sent(d, carry):
-            descriptor(d, False).wait_send()
+            descriptor(lax.rem(me + d, n), False).wait_send()
             return carry
 
         return start, arrived, sent
@@ -159,13 +189,11 @@
     b_start, b_arrived, b_sent = exchange(1, send_b, recv_b, True)
     c_start, c_arrived, c_sent = exchange(2, send_c, recv_c, False)
     e_start, e_arrived, e_sent = exchange(3, send_e, recv_e, True, tiles=True)
-    f_start, f_arrived, f_sent = exchange(4, send_f, recv_f, False, True)
     s_start, s_arrived, s_sent = exchange(5, send_s, recv_s, False, True)
-    g_start, g_arrived, g_sent = exchange(6, send_g, recv_g, False)
     h_start, h_arrived, h_sent = exchange(7, send_h, recv_h, True, tiles=True)
 
-    copies[0].wait()
-    copies[1].wait()
+    copies["tokens"].wait()
+    copies["attn_gain"].wait()
     x = tokens[...].astype(F32)
     normed = x * lax.rsqrt(jnp.mean(x * x, axis=-1, keepdims=True) + EPS) * attn_gain[...]
     normed = normed.astype(BF16)
@@ -173,8 +201,12 @@
         send_a[i] = normed[:, i * cols : (i + 1) * cols]
     recv_a[ep] = send_a[ep]
     pl.semaphore_wait(barrier, 2 * (n - 1))
-    lax.fori_loop(1, n, a_start, 0)
-
+    a_start()
+    for name in late:
+        copies[name].start()
+
+    for name in ("lengths", "groups", "members", "gates", "logits"):
+        copies[name].wait()
     rows_s[...] = jnp.zeros_like(rows_s)
     rows_s[0:1, 0:seqs] = lengths_ref[...].astype(F32)
     rows_s[1:2, 0:seqs] = groups_ref[...].astype(F32)
@@ -214,20 +246,19 @@
     combine = jnp.where((wide_ranks == wide_rank) & (wide_kind < 4), hit0 * share0 + hit1 * share1, 0.0)
 
     wait_all(a_arrived)
-    for i in (2, 3, 4):
-        copies[i].wait()
+    for name in ("wq", "wk", "wv"):
+        copies[name].wait()
     everyone = recv_a[...].reshape(n * seqs, cols)
     partial = jnp.dot(everyone, wqkv[...], preferred_element_type=F32)
     send_b[...] = partial.reshape(n, seqs, 3 * hd)
     recv_b[ep] = send_b[ep]
-    lax.fori_loop(1, n, b_start, 0)
+    b_start()
     wait_all(b_arrived)
     projected = jnp.sum(recv_b[...], axis=0).astype(BF16)
     query = projected[:, 0:hd]
     fresh_k = projected[:, hd : 2 * hd]
     fresh_v = projected[:, 2 * hd : 3 * hd]
-    fresh_k_ref[...] = fresh_k
-    fresh_v_ref[...] = fresh_v
+    out_ref[:, cols:] = projected[:, hd:]
 
     total_heads = n
     slope = jnp.float32(0.0)
@@ -243,14 +274,17 @@
     q4 = jnp.concatenate([q2, q2], axis=1)
     q4_seq = iota((both, 2 * hd), 0) % seqs
     q4_side = iota((both, 2 * hd), 1) // hd
-    copies[5].wait()
+    copies["keys"].wait()
 
     def score_step(p, acc):
         lhs = jnp.where(q4_seq == 2 * p + q4_side, q4, 0.0).astype(BF16)
         rhs = jnp.concatenate([keys[2 * p], keys[2 * p + 1]], axis=1)
         return acc + lax.dot_general(lhs, rhs, NT, preferred_element_type=F32)
 
-    old = lax.fori_loop(0, seqs // 2, score_step, jnp.zeros((both, cache), F32)) * scale
+    old = jnp.zeros((both, cache), F32)
+    for p in range(seqs // 2):
+        old = score_step(p, old)
+    old = old * scale
     count = jnp.concatenate([columns[:, 0:1], columns[:, 0:1]], axis=0)
     place = iota((both, cache), 1).astype(F32)
     old = jnp.where(place < count, old - slope * (count - place), -jnp.inf)
@@ -260,30 +294,32 @@
     norm = jnp.sum(e_old, axis=-1, keepdims=True) + e_new
     m_old = e_old / norm
     m_new = e_new / norm
-    lam = lam_ref[...]
+    lam = lam_h[0]
     weights = (m_old[:seqs] - lam * m_old[seqs:]).astype(BF16).astype(F32)
     w_new = (m_new[:seqs] - lam * m_new[seqs:]).astype(BF16).astype(F32)
     w_pair = iota((seqs, cache), 0) // 2
-    copies[6].wait()
+    copies["vals"].wait()
 
     def value_step(p, acc):
         lhs = jnp.where(w_pair == p, weights, 0.0).astype(BF16)
         rhs = jnp.concatenate([vals[2 * p], vals[2 * p + 1]], axis=1)
         return acc + jnp.dot(lhs, rhs, preferred_element_type=F32)
 
-    mix = lax.fori_loop(0, seqs // 2, value_step, jnp.zeros((seqs, 2 * hd), F32))
+    mix = jnp.zeros((seqs, 2 * hd), F32)
+    for p in range(seqs // 2):
+        mix = value_step(p, mix)
     head_mix = jnp.where(iota((seqs, hd), 0) % 2 == 0, mix[:, :hd], mix[:, hd:])
     head_mix = head_mix + w_new * fresh_v.astype(F32)
-    copies[7].wait()
+    copies["head_gain"].wait()
     head_out = head_mix * lax.rsqrt(jnp.mean(head_mix * head_mix, axis=-1, keepdims=True) + EPS)
     head_out = (head_out * head_gain[...]).astype(BF16)
 
-    copies[8].wait()
+    copies["wo"].wait()
     for i in range(n):
         term = jnp.dot(head_out, wo[:, i * cols : (i + 1) * cols], preferred_element_type=F32)
         send_c[i] = term.astype(BF16)
     recv_c[tp] = send_c[tp]
-    lax.fori_loop(1, n, c_start, 0)
+    c_start()
     wait_all(c_arrived)
     attn_sum = jnp.sum(recv_c[...].astype(F32), axis=0)
     own_cols = pl.ds(pl.multiple_of(tp * cols, cols), cols)
@@ -298,7 +334,7 @@
     send_e[...] = packed
     recv_e[pl.ds(pl.multiple_of(ep * 8, 8), 8), :] = send_e[pl.ds(pl.multiple_of(ep * 8, 8), 8), :]
 
-    lax.fori_loop(1, n, e_start, 0)
+    e_start()
     wait_all(e_arrived)
 
     def tile_row(ref, j):
@@ -308,32 +344,55 @@
         jnp.concatenate([tile_row(recv_e, 2 * r), tile_row(recv_e, 2 * r + 1)], axis=1) for r in range(2)
     ]
     slab = jnp.concatenate(token_rows, axis=0)
-    copies[9].wait()
+    copies["moe_gain"].wait()
     send_f[...] = (slab * moe_gain[:, own_cols]).astype(BF16)
     on_lane = iota((n, 128), 0) == iota((n, 128), 1)
     on_next = iota((n, 128), 0) + n == iota((n, 128), 1)
     stat = jnp.where(on_lane, tile_row(recv_e, 4), 0.0) + jnp.where(on_next, tile_row(recv_e, 5), 0.0)
-    send_s[...] = jnp.broadcast_to(jnp.sum(stat, axis=0, keepdims=True), (8, 128))
+    send_s[...] = jnp.sum(stat, axis=0, keepdims=True)
     recv_f[tp] = send_f[...]
     recv_s[tp] = send_s[...]
 
-    lax.fori_loop(1, n, s_start, 0)
-    lax.fori_loop(1, n, f_start, 0)
-    for i in (10, 11):
-        copies[i].wait()
+    partner = tp + 1 - 2 * lax.rem(tp, 2)
+    core = lax.rem(tp, 2)
+    chips = n // 2
+    chip = tp // 2
+    z_order = sorted(range(1, chips), key=lambda a: -min(a, chips - a))
+
+    def row_copy(source, slot, target, lane):
+        return pltpu.make_async_remote_copy(
+            src_ref=source,
+            dst_ref=recv_f.at[slot],
+            send_sem=ss.at[4, lane],
+            recv_sem=rs.at[4, slot],
+            device_id=(ep, target),
+            device_id_type=MESH,
+        )
+
+    def z_peer(a):
+        return lax.rem(chip + a, chips) * 2 + core
+
+    outgoing = [row_copy(send_f, tp, z_peer(a), a) for a in z_order]
+    outgoing.append(row_copy(send_f, tp, partner, 0))
+    for copy in outgoing:
+        copy.start()
+    s_start()
+    for a in reversed(z_order):
+        slot = z_peer(a)
+        row_copy(send_f, slot, slot, a).wait_recv()
+        copy = row_copy(recv_f.at[slot], slot, partner, chips + a)
+        copy.start()
+        outgoing.append(copy)
+    for name in ("wg", "wu"):
+        copies[name].wait()
     slots = 2 * n
-
-    def up_block(peer):
-        at = pl.ds(pl.multiple_of(peer * cols, cols), cols)
-        return jnp.dot(recv_f[peer], wgu[at, :], preferred_element_type=F32)
-
-    def up_step(d, acc):
-        f_arrived(d)
-        return acc + up_block(lax.rem(tp + d, n))
-
-    gate_up = lax.fori_loop(1, n, up_step, up_block(tp))
+    for a in range(chips):
+        slot = lax.rem(chip + a, chips) * 2 + 1 - core
+        row_copy(send_f, slot, partner, a).wait_recv()
+    everything = jnp.concatenate([recv_f[i] for i in range(n)], axis=1)
+    gate_up = jnp.dot(everything, wgu[...], preferred_element_type=F32)
     wait_all(s_arrived)
-    stats = jnp.sum(recv_s[...], axis=0)
+    stats = jnp.broadcast_to(jnp.sum(recv_s[...], axis=0), (8, 128))
     eye_slots = (iota((slots, 128), 0) == iota((slots, 128), 1)).astype(F32)
     sums = exact_dot(eye_slots, stats, NT)[:, 0:1]
     norm_scale = lax.rsqrt(sums / width + EPS)
@@ -341,13 +400,46 @@
     upper = gate_up[:, hd:] * norm_scale
     hidden = (gate / (1.0 + jnp.exp(-gate)) * upper).astype(BF16)
 
-    copies[12].wait()
-    for i in range(n):
-        down = jnp.dot(hidden, wd[:, i * cols : (i + 1) * cols], preferred_element_type=F32)
-        send_g[i] = down.astype(BF16)
-    recv_g[tp] = send_g[tp]
-    lax.fori_loop(1, n, g_start, 0)
-    wait_all(g_arrived)
+    copies["wd"].wait()
+
+    def down_block(z, c):
+        at = pl.ds(pl.multiple_of((2 * z + c) * cols, cols), cols)
+        return jnp.dot(hidden, wd[:, at], preferred_element_type=F32)
+
+    for z in range(chips):
+        pair_out[z] = down_block(z, 1 - core).astype(BF16)
+    pair_copy = pltpu.make_async_remote_copy(
+        src_ref=pair_out,
+        dst_ref=pair_in,
+        send_sem=ss.at[6, 0],
+        recv_sem=rs.at[6, 0],
+        device_id=(ep, partner),
+        device_id_type=MESH,
+    )
+    pair_copy.start()
+    outgoing.append(pair_copy)
+    for z in range(chips):
+        pair_own[z] = down_block(z, core)
+    pair_copy.wait_recv()
+    send_g[...] = (pair_own[...] + pair_in[...].astype(F32)).astype(BF16)
+    recv_g[chip] = send_g[chip]
+
+    def sum_copy(a, slot):
+        return pltpu.make_async_remote_copy(
+            src_ref=send_g.at[lax.rem(chip + a, chips)],
+            dst_ref=recv_g.at[slot],
+            send_sem=ss.at[6, a],
+            recv_sem=rs.at[6, 1 + slot],
+            device_id=(ep, z_peer(a)),
+            device_id_type=MESH,
+        )
+
+    for a in z_order:
+        copy = sum_copy(a, chip)
+        copy.start()
+        outgoing.append(copy)
+    for a in reversed(z_order):
+        sum_copy(a, lax.rem(chip + a, chips)).wait_recv()
     expert_out = jnp.sum(recv_g[...].astype(F32), axis=0).astype(BF16).astype(F32)
 
     send_h[...] = jnp.zeros_like(send_h)
@@ -355,14 +447,29 @@
         for h in range(2):
             send_h[pl.ds(2 * r + h, n, stride=8), :] = expert_out[r * n : (r + 1) * n, h * 128 : (h + 1) * 128]
     recv_h[pl.ds(pl.multiple_of(ep * 8, 8), 8), :] = send_h[pl.ds(pl.multiple_of(ep * 8, 8), 8), :]
-    lax.fori_loop(1, n, h_start, 0)
+    h_start()
     wait_all(h_arrived)
     back = recv_h[...]
     routed = [exact_dot(jnp.where(wide_kind % 2 == h, combine, 0.0), back) for h in range(2)]
-    mixed_ref[...] = (resid + jnp.concatenate(routed, axis=1)).astype(BF16)
-
-    for sent in (a_sent, b_sent, c_sent, e_sent, f_sent, s_sent, g_sent, h_sent):
+    out_ref[:, :cols] = (resid + jnp.concatenate(routed, axis=1)).astype(BF16)
+
+    for sent in (a_sent, b_sent, c_sent, e_sent, s_sent, h_sent):
         lax.fori_loop(1, n, sent, 0)
+    for copy in outgoing:
+        copy.wait_send()
+
+
+def unpack_kernel(packed_ref, mixed_ref, fresh_k_ref, fresh_v_ref, sems):
+    copies = []
+    at = 0
+    for i, ref in enumerate((mixed_ref, fresh_k_ref, fresh_v_ref)):
+        size = ref.shape[1]
+        copies.append(pltpu.make_async_copy(packed_ref.at[:, pl.ds(at, size)], ref, sems.at[i]))
+        at += size
+    for copy in copies:
+        copy.start()
+    for copy in copies:
+        copy.wait()
 
 
 def on_device(n, *args):
@@ -378,7 +485,7 @@
         w_query,
         w_key,
         w_value,
-        mix_lambda.reshape(1, 1),
+        mix_lambda,
         head_gain.reshape(1, hd),
         w_output,
         cache_keys,
@@ -393,13 +500,18 @@
         w_exp_up,
         w_exp_down,
     )
-    small = (5, 10, 12, 13, 14, 15)
     vmem = pl.BlockSpec(memory_space=pltpu.VMEM)
     hbm = pl.BlockSpec(memory_space=pl.ANY)
     scratch = [
         pltpu.VMEM((seqs, width), BF16),
         pltpu.VMEM((1, width), F32),
         pltpu.VMEM((w_query.shape[0], 3 * hd), BF16),
+        pltpu.SMEM((1,), F32),
+        pltpu.VMEM((1, seqs), jnp.int32),
+        pltpu.VMEM((1, seqs), jnp.int32),
+        pltpu.VMEM((2, seqs), jnp.int32),
+        pltpu.VMEM((1, seqs), F32),
+        pltpu.VMEM((2, seqs), F32),
         pltpu.VMEM((1, hd), F32),
         pltpu.VMEM((hd, width), BF16),
         pltpu.VMEM((seqs, cache, hd), BF16),
@@ -418,29 +530,40 @@
         pltpu.VMEM((8 * n, 128), F32),
         pltpu.VMEM((2 * n, cols), BF16),
         pltpu.VMEM((n, 2 * n, cols), BF16),
-        pltpu.VMEM((8, 128), F32),
-        pltpu.VMEM((n, 8, 128), F32),
-        pltpu.VMEM((n, 2 * n, cols), BF16),
-        pltpu.VMEM((n, 2 * n, cols), BF16),
+        pltpu.VMEM((1, 128), F32),
+        pltpu.VMEM((n, 1, 128), F32),
+        pltpu.VMEM((n // 2, 2 * n, cols), BF16),
+        pltpu.VMEM((n // 2, 2 * n, cols), BF16),
+        pltpu.VMEM((n // 2, 2 * n, cols), F32),
+        pltpu.VMEM((n // 2, 2 * n, cols), BF16),
+        pltpu.VMEM((n // 2, 2 * n, cols), BF16),
         pltpu.VMEM((8 * n, 128), F32),
         pltpu.VMEM((8 * n, 128), F32),
-        pltpu.SemaphoreType.DMA((13,)),
+        pltpu.SemaphoreType.DMA((19,)),
         pltpu.SemaphoreType.DMA((8, n)),
         pltpu.SemaphoreType.DMA((8, n)),
     ]
+    packed = pl.pallas_call(
+        functools.partial(layer_kernel, n),
+        out_shape=pltpu.VMEM((seqs, cols + 2 * hd), BF16),
+        in_specs=[pl.BlockSpec(memory_space=pltpu.SMEM) if i == 5 else hbm for i in range(len(operands))],
+        out_specs=vmem,
+        scratch_shapes=scratch,
+        compiler_params=pltpu.CompilerParams(collective_id=0, has_side_effects=True),
+        name="layer",
+    )(*operands)
     return pl.pallas_call(
-        functools.partial(layer_kernel, n),
+        unpack_kernel,
         out_shape=(
             jax.ShapeDtypeStruct((seqs, cols), BF16),
             jax.ShapeDtypeStruct((seqs, hd), BF16),
             jax.ShapeDtypeStruct((seqs, hd), BF16),
         ),
-        in_specs=[vmem if i in small else hbm for i in range(len(operands))],
-        out_specs=(vmem, vmem, vmem),
-        scratch_shapes=scratch,
-        compiler_params=pltpu.CompilerParams(collective_id=0, has_side_effects=True),
-        name="layer",
-    )(*operands)
+        in_specs=[vmem],
+        out_specs=(hbm, hbm, hbm),
+        scratch_shapes=[pltpu.SemaphoreType.DMA((3,))],
+        name="unpack",
+    )(pltpu.with_memory_space_constraint(packed, pltpu.VMEM))
 
 
 def solution(mesh):

time: 71.5 us -> 57.7 us (0.81); the launches traced: 70.1 us -> 57.2 us
  Pallas kernels: 65 us -> 55.9 us
  local copies, waits for them, and re-layouts: 3.83 us -> 0 us
    pallas_call x1 -> x2, Pallas kernels: 65 us -> 55.9 us  [the longest x1 55.3 us: on_device(): pl.pallas_call(functools.partial(layer_kernel, n), out_shape=pltpu.VMEM((...]
    unnamed x3 -> x0, local copies, waits for them, and re-layouts: 3.83 us -> none
where the time goes in v2:
time: 57.7 us; the launch traced here: 57.2 us
  Pallas kernels  55.9 us (97%)
  between operations  1.29 us (2%)
    pallas_call x1, Pallas kernels, on_device(): pl.pallas_call(functools.partial(layer_kernel, n), out_shape=pltpu.VMEM((...  55.3 us

profile of v2, /device:TPU:8, one launch (start us, length us, event | category | flops | bytes accessed | tf_op | source)
XLA Modules:
  0.0 57.2 jit_solution(13836118198601835656)
XLA Ops:
  1.3 55.3 %layer.1.packed_ref = bf16[16,512]{1,0:T(8,128)(2,1)S(1)} custom-call(bf16[16,4096]{1,0:T(8,128)(2,1)} %tokens_h.1, f32[1,4096]{1,0:T(1,128)} %bitcast.8, bf16[256,128]{1,0:T(8,128)(2,1)} %wq_h.1, bf16[256,128]{1,0:T(8,128)(2,1)} %wk_h.1, bf16[256,128]{1,0:T(8,128)(2,1)} %wv_h.1, f32[1]{0:T(128)S(6)} %copy.22.lam_h, f32[1,128]{1,0:T(1,128)} %bitcast.12, ...), custom_call_target="tpu_custom_call" | custom-call | tf_op jit(solution)/shard_map/layer/pallas_call | solution.py:546
  56.6 0.6 %unpack.1 = (bf16[16,256]{1,0:T(8,128)(2,1)}, bf16[16,128]{1,0:T(8,128)(2,1)}, bf16[16,128]{1,0:T(8,128)(2,1)}) custom-call(bf16[16,512]{1,0:T(8,128)(2,1)S(1)} %layer.1.packed_ref), custom_call_target="tpu_custom_call" | custom-call | tf_op jit(solution)/shard_map/unpack/pallas_call | solution.py:555

commit v3 on v2

--- a/solution.py
+++ b/solution.py
@@ -67,6 +67,9 @@
     recv_a,
     send_b,
     recv_b,
+    term_out,
+    term_in,
+    term_own,
     send_c,
     recv_c,
     send_e,
@@ -74,6 +77,8 @@
     send_f,
     recv_f,
     send_s,
+    stat_in,
+    pair_s,
     recv_s,
     pair_out,
     pair_in,
@@ -88,6 +93,10 @@
 ):
     ep = lax.axis_index("ep")
     tp = lax.axis_index("tp")
+    core = lax.rem(tp, 2)
+    partner = tp + 1 - 2 * core
+    chips = n // 2
+    chip = tp // 2
     width = tokens_h.shape[1]
     cols = width // n
     seqs = tokens_h.shape[0]
@@ -95,14 +104,21 @@
     half = hd // 2
     cache = keys_h.shape[1]
 
-    barrier = pltpu.get_barrier_semaphore()
-
-    def greet(d, carry):
-        pl.semaphore_signal(barrier, inc=1, device_id=(lax.rem(ep + d, n), tp), device_id_type=MESH)
-        pl.semaphore_signal(barrier, inc=1, device_id=(ep, lax.rem(tp + d, n)), device_id_type=MESH)
-        return carry
-
-    lax.fori_loop(1, n, greet, 0)
+    side = 4
+    ep_offsets = [(a, b) for a in range(side) for b in range(n // side) if (a, b) != (0, 0)]
+
+    def ep_hops(o):
+        return min(o[0], side - o[0]) + min(o[1], n // side - o[1])
+
+    def ep_peer(o):
+        return lax.rem(ep // side + o[0], side) * side + lax.rem(ep % side + o[1], side)
+
+    ep_offsets.sort(key=lambda o: -ep_hops(o))
+    ep_peers = [ep_peer(o) for o in ep_offsets]
+    z_order = sorted(range(1, chips), key=lambda a: -min(a, chips - a))
+
+    def z_peer(a):
+        return lax.rem(chip + a, chips) * 2 + core
 
     loads = {
         "tokens": (tokens_h, tokens),
@@ -128,69 +144,97 @@
         name: pltpu.make_async_copy(source, target, load_sem.at[i])
         for i, (name, (source, target)) in enumerate(loads.items())
     }
+    copies["tokens"].start()
+    copies["attn_gain"].start()
+
+    barrier = pltpu.get_barrier_semaphore()
+    for peer in ep_peers:
+        pl.semaphore_signal(barrier, inc=1, device_id=(peer, tp), device_id_type=MESH)
+    for a in z_order:
+        pl.semaphore_signal(barrier, inc=1, device_id=(ep, z_peer(a)), device_id_type=MESH)
+    pl.semaphore_signal(barrier, inc=1, device_id=(ep, partner), device_id_type=MESH)
+
     late = ("keys", "vals", "wo", "wg", "wu", "wd")
     for name, copy in copies.items():
-        if name not in late:
+        if name not in late + ("tokens", "attn_gain"):
             copy.start()
 
-    def far_first(over_ep):
-        if over_ep:
-            side = 4
-            offsets = [(a, b) for a in range(side) for b in range(n // side) if (a, b) != (0, 0)]
-            offsets.sort(key=lambda o: -(min(o[0], side - o[0]) + min(o[1], n // side - o[1])))
-            for a, b in offsets:
-                yield lax.rem(ep // side + a, side) * side + lax.rem(ep % side + b, side)
-        else:
-            chips = n // 2
-            offsets = [(a, b) for a in range(chips) for b in range(2) if (a, b) != (0, 0)]
-            offsets.sort(key=lambda o: -min(o[0], chips - o[0]))
-            for a, b in offsets:
-                yield lax.rem(tp // 2 + a, chips) * 2 + lax.rem(tp % 2 + b, 2)
-
-    def block(ref, i, tiles):
-        return ref.at[pl.ds(pl.multiple_of(i * 8, 8), 8), :] if tiles else ref.at[i]
-
-    def exchange(phase, send, recv, over_ep, whole=False, tiles=False):
-        me = ep if over_ep else tp
+    def exchange(phase, send, recv, tile_rows=None):
+        def block(ref, i):
+            return ref.at[i] if tile_rows is None else ref.at[pl.ds(pl.multiple_of(i * 8, 8), tile_rows), :]
 
         def descriptor(peer, incoming):
-            slot = peer if incoming else me
-            target = (peer, tp) if over_ep else (ep, peer)
             return pltpu.make_async_remote_copy(
-                src_ref=send if whole else block(send, peer, tiles),
-                dst_ref=block(recv, slot, tiles),
+                src_ref=block(send, peer),
+                dst_ref=block(recv, peer if incoming else ep),
                 send_sem=ss.at[phase, peer],
-                recv_sem=rs.at[phase, slot],
-                device_id=target,
+                recv_sem=rs.at[phase, peer if incoming else ep],
+                device_id=(peer, tp),
                 device_id_type=MESH,
             )
 
-        def start():
-            for peer in far_first(over_ep):
+        def start(peers):
+            for peer in peers:
                 descriptor(peer, False).start()
 
-        def arrived(d):
-            descriptor(lax.rem(me + d, n), True).wait_recv()
+        def arrived(peer):
+            descriptor(peer, True).wait_recv()
 
         def sent(d, carry):
-            descriptor(lax.rem(me + d, n), False).wait_send()
+            descriptor(lax.rem(ep + d, n), False).wait_send()
             return carry
 
         return start, arrived, sent
 
     def wait_all(arrived):
         def body(d, carry):
-            arrived(d)
+            arrived(lax.rem(ep + d, n))
             return carry
 
         lax.fori_loop(1, n, body, 0)
 
-    a_start, a_arrived, a_sent = exchange(0, send_a, recv_a, True)
-    b_start, b_arrived, b_sent = exchange(1, send_b, recv_b, True)
-    c_start, c_arrived, c_sent = exchange(2, send_c, recv_c, False)
-    e_start, e_arrived, e_sent = exchange(3, send_e, recv_e, True, tiles=True)
-    s_start, s_arrived, s_sent = exchange(5, send_s, recv_s, False, True)
-    h_start, h_arrived, h_sent = exchange(7, send_h, recv_h, True, tiles=True)
+    outgoing = []
+
+    def to_partner(phase, source, target):
+        copy = pltpu.make_async_remote_copy(
+            src_ref=source,
+            dst_ref=target,
+            send_sem=ss.at[phase, 0],
+            recv_sem=rs.at[phase, n - 1],
+            device_id=(ep, partner),
+            device_id_type=MESH,
+        )
+        copy.start()
+        outgoing.append(copy)
+        return copy
+
+    def along_z(phase, source, recv):
+        def descriptor(a, slot):
+            return pltpu.make_async_remote_copy(
+                src_ref=source(lax.rem(chip + a, chips)),
+                dst_ref=recv.at[slot],
+                send_sem=ss.at[phase, a],
+                recv_sem=rs.at[phase, slot],
+                device_id=(ep, z_peer(a)),
+                device_id_type=MESH,
+            )
+
+        for a in z_order:
+            copy = descriptor(a, chip)
+            copy.start()
+            outgoing.append(copy)
+
+        def wait():
+            for a in reversed(z_order):
+                descriptor(a, lax.rem(chip + a, chips)).wait_recv()
+
+        return wait
+
+    a_start, a_arrived, a_sent = exchange(0, send_a, recv_a)
+    b_start, b_arrived, b_sent = exchange(1, send_b, recv_b)
+    e_start, e_arrived, e_sent = exchange(3, send_e, recv_e, 6)
+    h_start, h_arrived, h_sent = exchange(7, send_h, recv_h, 4)
+    recv_h[...] = jnp.zeros_like(recv_h)
 
     copies["tokens"].wait()
     copies["attn_gain"].wait()
@@ -200,8 +244,8 @@
     for i in range(n):
         send_a[i] = normed[:, i * cols : (i + 1) * cols]
     recv_a[ep] = send_a[ep]
-    pl.semaphore_wait(barrier, 2 * (n - 1))
-    a_start()
+    pl.semaphore_wait(barrier, n - 1 + chips)
+    a_start(ep_peers)
     for name in late:
         copies[name].start()
 
@@ -235,6 +279,10 @@
     before = (iota((seqs, seqs), 0) < iota((seqs, seqs), 1)).astype(F32)
     rank = exact_dot(chosen, before)
     dispatch = jnp.where((rank == tall_rank) & (tall_kind < 6), chosen, 0.0)
+    first = (tall_kind == 0) | (tall_kind == 2)
+    second = (tall_kind == 1) | (tall_kind == 3)
+    kinds = [jnp.where(kind, dispatch, 0.0) for kind in (first, second, tall_kind >= 4)]
+    routes = jnp.concatenate(kinds * 3, axis=1).astype(BF16)
     wide_col = iota((seqs, tall), 1)
     wide_expert = (wide_col // 8).astype(F32)
     wide_kind = wide_col % 8
@@ -245,14 +293,23 @@
     wide_ranks = exact_dot(after, hit0 + hit1)
     combine = jnp.where((wide_ranks == wide_rank) & (wide_kind < 4), hit0 * share0 + hit1 * share1, 0.0)
 
-    wait_all(a_arrived)
+    parts = []
+    for h in range(2):
+        rest = jnp.where(wide_kind % 2 == h, combine, 0.0)
+        for _ in range(3):
+            part = rest.astype(BF16)
+            parts.append(part)
+            rest = rest - part.astype(F32)
+    shares = jnp.concatenate(parts, axis=0)
+
     for name in ("wq", "wk", "wv"):
         copies[name].wait()
+    wait_all(a_arrived)
     everyone = recv_a[...].reshape(n * seqs, cols)
     partial = jnp.dot(everyone, wqkv[...], preferred_element_type=F32)
     send_b[...] = partial.reshape(n, seqs, 3 * hd)
+    b_start(ep_peers)
     recv_b[ep] = send_b[ep]
-    b_start()
     wait_all(b_arrived)
     projected = jnp.sum(recv_b[...], axis=0).astype(BF16)
     query = projected[:, 0:hd]
@@ -265,76 +322,90 @@
     for h in range(total_heads):
         slope = jnp.where(tp == h, jnp.float32(2.0 ** (-8.0 * (h + 1.0) / total_heads)), slope)
     scale = half ** (-0.5)
-    both = 2 * seqs
-    q2 = jnp.concatenate([query, query], axis=0).astype(F32)
-    k2 = jnp.concatenate([fresh_k, fresh_k], axis=0).astype(F32)
-    own_map = (iota((both, hd), 0) // seqs) == (iota((both, hd), 1) // half)
-    q2 = jnp.where(own_map, q2, 0.0)
-    new = jnp.sum(q2 * k2, axis=-1, keepdims=True) * scale
-    q4 = jnp.concatenate([q2, q2], axis=1)
-    q4_seq = iota((both, 2 * hd), 0) % seqs
+    some = seqs // 2
+    both = 2 * some
+    q_all = query.astype(F32)
+    k_all = fresh_k.astype(F32)
+    v_all = fresh_v.astype(F32)
+    own_map = (iota((both, hd), 0) // some) == (iota((both, hd), 1) // half)
+    q4_seq = iota((both, 2 * hd), 0) % some
     q4_side = iota((both, 2 * hd), 1) // hd
+    place = iota((both, cache), 1).astype(F32)
+    mix_seq = iota((some, hd), 0)
     copies["keys"].wait()
-
-    def score_step(p, acc):
-        lhs = jnp.where(q4_seq == 2 * p + q4_side, q4, 0.0).astype(BF16)
-        rhs = jnp.concatenate([keys[2 * p], keys[2 * p + 1]], axis=1)
-        return acc + lax.dot_general(lhs, rhs, NT, preferred_element_type=F32)
-
-    old = jnp.zeros((both, cache), F32)
-    for p in range(seqs // 2):
-        old = score_step(p, old)
-    old = old * scale
-    count = jnp.concatenate([columns[:, 0:1], columns[:, 0:1]], axis=0)
-    place = iota((both, cache), 1).astype(F32)
-    old = jnp.where(place < count, old - slope * (count - place), -jnp.inf)
-    top = jnp.maximum(jnp.max(old, axis=-1, keepdims=True), new)
-    e_old = jnp.exp(old - top)
-    e_new = jnp.exp(new - top)
-    norm = jnp.sum(e_old, axis=-1, keepdims=True) + e_new
-    m_old = e_old / norm
-    m_new = e_new / norm
+    scores = []
+    for part in range(2):
+        at = slice(part * some, (part + 1) * some)
+        q2 = jnp.where(own_map, jnp.concatenate([q_all[at], q_all[at]], axis=0), 0.0)
+        q4 = jnp.concatenate([q2, q2], axis=1)
+        old = jnp.zeros((both, cache), F32)
+        for p in range(some // 2):
+            lhs = jnp.where(q4_seq == 2 * p + q4_side, q4, 0.0).astype(BF16)
+            b0 = part * some + 2 * p
+            rhs = jnp.concatenate([keys[b0], keys[b0 + 1]], axis=1)
+            old = old + lax.dot_general(lhs, rhs, NT, preferred_element_type=F32)
+        scores.append((q2, old * scale))
+    copies["vals"].wait()
     lam = lam_h[0]
-    weights = (m_old[:seqs] - lam * m_old[seqs:]).astype(BF16).astype(F32)
-    w_new = (m_new[:seqs] - lam * m_new[seqs:]).astype(BF16).astype(F32)
-    w_pair = iota((seqs, cache), 0) // 2
-    copies["vals"].wait()
-
-    def value_step(p, acc):
-        lhs = jnp.where(w_pair == p, weights, 0.0).astype(BF16)
-        rhs = jnp.concatenate([vals[2 * p], vals[2 * p + 1]], axis=1)
-        return acc + jnp.dot(lhs, rhs, preferred_element_type=F32)
-
-    mix = jnp.zeros((seqs, 2 * hd), F32)
-    for p in range(seqs // 2):
-        mix = value_step(p, mix)
-    head_mix = jnp.where(iota((seqs, hd), 0) % 2 == 0, mix[:, :hd], mix[:, hd:])
-    head_mix = head_mix + w_new * fresh_v.astype(F32)
+    mixes = []
+    for part, (q2, old) in enumerate(scores):
+        at = slice(part * some, (part + 1) * some)
+        new = jnp.sum(q2 * jnp.concatenate([k_all[at], k_all[at]], axis=0), axis=-1, keepdims=True) * scale
+        count = jnp.concatenate([columns[at, 0:1], columns[at, 0:1]], axis=0)
+        old = jnp.where(place < count, old - slope * (count - place), -jnp.inf)
+        top = jnp.maximum(jnp.max(old, axis=-1, keepdims=True), new)
+        e_old = jnp.exp(old - top)
+        e_new = jnp.exp(new - top)
+        norm = jnp.sum(e_old, axis=-1, keepdims=True) + e_new
+        m_old = e_old / norm
+        m_new = e_new / norm
+        weights = (m_old[:some] - lam * m_old[some:]).astype(BF16)
+        w_new = (m_new[:some] - lam * m_new[some:]).astype(BF16).astype(F32)
+        mix = w_new * v_all[at]
+        for p in range(some // 2):
+            b0 = part * some + 2 * p
+            pair = jnp.concatenate([vals[b0], vals[b0 + 1]], axis=1)
+            both_mix = jnp.dot(weights, pair, preferred_element_type=F32)
+            mix = mix + jnp.where(mix_seq == 2 * p, both_mix[:, :hd], 0.0)
+            mix = mix + jnp.where(mix_seq == 2 * p + 1, both_mix[:, hd:], 0.0)
+        mixes.append(mix)
+    head_mix = jnp.concatenate(mixes, axis=0)
     copies["head_gain"].wait()
     head_out = head_mix * lax.rsqrt(jnp.mean(head_mix * head_mix, axis=-1, keepdims=True) + EPS)
     head_out = (head_out * head_gain[...]).astype(BF16)
 
     copies["wo"].wait()
-    for i in range(n):
-        term = jnp.dot(head_out, wo[:, i * cols : (i + 1) * cols], preferred_element_type=F32)
-        send_c[i] = term.astype(BF16)
-    recv_c[tp] = send_c[tp]
-    c_start()
-    wait_all(c_arrived)
+
+    def term_block(z, c):
+        at = pl.ds(pl.multiple_of((2 * z + c) * cols, cols), cols)
+        return jnp.dot(head_out, wo[:, at], preferred_element_type=F32).astype(BF16)
+
+    for z in range(chips):
+        term_out[z] = term_block(z, 1 - core)
+    term_copy = to_partner(2, term_out, term_in)
+    for z in range(chips):
+        term_own[z] = term_block(z, core).astype(F32)
+    term_copy.wait_recv()
+    send_c[...] = (term_own[...] + term_in[...].astype(F32)).astype(BF16)
+    c_wait = along_z(2, lambda i: send_c.at[i], recv_c)
+    recv_c[chip] = send_c[chip]
+    c_wait()
     attn_sum = jnp.sum(recv_c[...].astype(F32), axis=0)
     own_cols = pl.ds(pl.multiple_of(tp * cols, cols), cols)
     resid = tokens[:, own_cols].astype(F32) + attn_sum
 
     squares = jnp.broadcast_to(jnp.sum(resid * resid, axis=-1, keepdims=True), (seqs, 128))
-    first = (tall_kind == 0) | (tall_kind == 2)
-    second = (tall_kind == 1) | (tall_kind == 3)
-    packed = exact_dot(jnp.where(first, dispatch, 0.0), resid[:, :128])
-    packed += exact_dot(jnp.where(second, dispatch, 0.0), resid[:, 128:])
-    packed += exact_dot(jnp.where(tall_kind >= 4, dispatch, 0.0), squares)
+    rest = [resid[:, :128], resid[:, 128:], squares]
+    parts = []
+    for _ in range(3):
+        part = [r.astype(BF16) for r in rest]
+        rest = [r - p.astype(F32) for r, p in zip(rest, part)]
+        parts += part
+    packed = jnp.dot(routes, jnp.concatenate(parts, axis=0), preferred_element_type=F32)
     send_e[...] = packed
     recv_e[pl.ds(pl.multiple_of(ep * 8, 8), 8), :] = send_e[pl.ds(pl.multiple_of(ep * 8, 8), 8), :]
 
-    e_start()
+    e_start(ep_peers)
     wait_all(e_arrived)
 
     def tile_row(ref, j):
@@ -351,13 +422,9 @@
     stat = jnp.where(on_lane, tile_row(recv_e, 4), 0.0) + jnp.where(on_next, tile_row(recv_e, 5), 0.0)
     send_s[...] = jnp.sum(stat, axis=0, keepdims=True)
     recv_f[tp] = send_f[...]
-    recv_s[tp] = send_s[...]
-
-    partner = tp + 1 - 2 * lax.rem(tp, 2)
-    core = lax.rem(tp, 2)
-    chips = n // 2
-    chip = tp // 2
-    z_order = sorted(range(1, chips), key=lambda a: -min(a, chips - a))
+
+    recv_s[chip] = send_s[...]
+    s_wait = along_z(5, lambda i: send_s, recv_s)
 
     def row_copy(source, slot, target, lane):
         return pltpu.make_async_remote_copy(
@@ -369,30 +436,30 @@
             device_id_type=MESH,
         )
 
-    def z_peer(a):
-        return lax.rem(chip + a, chips) * 2 + core
-
-    outgoing = [row_copy(send_f, tp, z_peer(a), a) for a in z_order]
-    outgoing.append(row_copy(send_f, tp, partner, 0))
-    for copy in outgoing:
+    rows_out = [row_copy(send_f, tp, z_peer(a), a) for a in z_order]
+    rows_out.append(row_copy(send_f, tp, partner, 0))
+    for copy in rows_out:
         copy.start()
-    s_start()
     for a in reversed(z_order):
         slot = z_peer(a)
         row_copy(send_f, slot, slot, a).wait_recv()
         copy = row_copy(recv_f.at[slot], slot, partner, chips + a)
         copy.start()
-        outgoing.append(copy)
+        rows_out.append(copy)
+    outgoing.extend(rows_out)
     for name in ("wg", "wu"):
         copies[name].wait()
     slots = 2 * n
+    s_wait()
+    pair_s[...] = jnp.sum(recv_s[...], axis=0)
+    stat_copy = to_partner(5, pair_s, stat_in)
     for a in range(chips):
         slot = lax.rem(chip + a, chips) * 2 + 1 - core
         row_copy(send_f, slot, partner, a).wait_recv()
     everything = jnp.concatenate([recv_f[i] for i in range(n)], axis=1)
     gate_up = jnp.dot(everything, wgu[...], preferred_element_type=F32)
-    wait_all(s_arrived)
-    stats = jnp.broadcast_to(jnp.sum(recv_s[...], axis=0), (8, 128))
+    stat_copy.wait_recv()
+    stats = jnp.broadcast_to(pair_s[...] + stat_in[...], (8, 128))
     eye_slots = (iota((slots, 128), 0) == iota((slots, 128), 1)).astype(F32)
     sums = exact_dot(eye_slots, stats, NT)[:, 0:1]
     norm_scale = lax.rsqrt(sums / width + EPS)
@@ -408,52 +475,27 @@
 
     for z in range(chips):
         pair_out[z] = down_block(z, 1 - core).astype(BF16)
-    pair_copy = pltpu.make_async_remote_copy(
-        src_ref=pair_out,
-        dst_ref=pair_in,
-        send_sem=ss.at[6, 0],
-        recv_sem=rs.at[6, 0],
-        device_id=(ep, partner),
-        device_id_type=MESH,
-    )
-    pair_copy.start()
-    outgoing.append(pair_copy)
+    pair_copy = to_partner(6, pair_out, pair_in)
     for z in range(chips):
         pair_own[z] = down_block(z, core)
     pair_copy.wait_recv()
     send_g[...] = (pair_own[...] + pair_in[...].astype(F32)).astype(BF16)
+    g_wait = along_z(6, lambda i: send_g.at[i], recv_g)
     recv_g[chip] = send_g[chip]
-
-    def sum_copy(a, slot):
-        return pltpu.make_async_remote_copy(
-            src_ref=send_g.at[lax.rem(chip + a, chips)],
-            dst_ref=recv_g.at[slot],
-            send_sem=ss.at[6, a],
-            recv_sem=rs.at[6, 1 + slot],
-            device_id=(ep, z_peer(a)),
-            device_id_type=MESH,
-        )
-
-    for a in z_order:
-        copy = sum_copy(a, chip)
-        copy.start()
-        outgoing.append(copy)
-    for a in reversed(z_order):
-        sum_copy(a, lax.rem(chip + a, chips)).wait_recv()
+    g_wait()
     expert_out = jnp.sum(recv_g[...].astype(F32), axis=0).astype(BF16).astype(F32)
 
-    send_h[...] = jnp.zeros_like(send_h)
     for r in range(2):
         for h in range(2):
             send_h[pl.ds(2 * r + h, n, stride=8), :] = expert_out[r * n : (r + 1) * n, h * 128 : (h + 1) * 128]
-    recv_h[pl.ds(pl.multiple_of(ep * 8, 8), 8), :] = send_h[pl.ds(pl.multiple_of(ep * 8, 8), 8), :]
-    h_start()
+    recv_h[pl.ds(pl.multiple_of(ep * 8, 8), 4), :] = send_h[pl.ds(pl.multiple_of(ep * 8, 8), 4), :]
+    h_start(ep_peers)
     wait_all(h_arrived)
-    back = recv_h[...]
-    routed = [exact_dot(jnp.where(wide_kind % 2 == h, combine, 0.0), back) for h in range(2)]
+    back = jnp.dot(shares, recv_h[...].astype(BF16), preferred_element_type=F32)
+    routed = [sum(back[(3 * h + i) * seqs : (3 * h + i + 1) * seqs] for i in range(3)) for h in range(2)]
     out_ref[:, :cols] = (resid + jnp.concatenate(routed, axis=1)).astype(BF16)
 
-    for sent in (a_sent, b_sent, c_sent, e_sent, s_sent, h_sent):
+    for sent in (a_sent, b_sent, e_sent, h_sent):
         lax.fori_loop(1, n, sent, 0)
     for copy in outgoing:
         copy.wait_send()
@@ -524,14 +566,19 @@
         pltpu.VMEM((n, seqs, cols), BF16),
         pltpu.VMEM((n, seqs, 3 * hd), F32),
         pltpu.VMEM((n, seqs, 3 * hd), F32),
-        pltpu.VMEM((n, seqs, cols), BF16),
-        pltpu.VMEM((n, seqs, cols), BF16),
+        pltpu.VMEM((n // 2, seqs, cols), BF16),
+        pltpu.VMEM((n // 2, seqs, cols), BF16),
+        pltpu.VMEM((n // 2, seqs, cols), F32),
+        pltpu.VMEM((n // 2, seqs, cols), BF16),
+        pltpu.VMEM((n // 2, seqs, cols), BF16),
         pltpu.VMEM((8 * n, 128), F32),
         pltpu.VMEM((8 * n, 128), F32),
         pltpu.VMEM((2 * n, cols), BF16),
         pltpu.VMEM((n, 2 * n, cols), BF16),
         pltpu.VMEM((1, 128), F32),
-        pltpu.VMEM((n, 1, 128), F32),
+        pltpu.VMEM((1, 128), F32),
+        pltpu.VMEM((1, 128), F32),
+        pltpu.VMEM((n // 2, 1, 128), F32),
         pltpu.VMEM((n // 2, 2 * n, cols), BF16),
         pltpu.VMEM((n // 2, 2 * n, cols), BF16),
         pltpu.VMEM((n // 2, 2 * n, cols), F32),

time: 57.7 us -> 55.8 us (0.967)
  Pallas kernels: 55.9 us -> 54.4 us
    pallas_call x1, Pallas kernels: 55.3 us -> 53.7 us  [on_device(): pl.pallas_call(functools.partial(layer_kernel, n), out_shape=pltpu.VMEM((...]
where the time goes in v3:
time: 55.8 us; the launch traced here: 55.7 us
  Pallas kernels  54.4 us (97%)
  between operations  1.29 us (2%)
    pallas_call x1, Pallas kernels, on_device(): pl.pallas_call(functools.partial(layer_kernel, n), out_shape=pltpu.VMEM((...  53.7 us

profile of v3, /device:TPU:8, one launch (start us, length us, event | category | flops | bytes accessed | tf_op | source)
XLA Modules:
  0.0 55.7 jit_solution(11382622861145140569)
XLA Ops:
  1.3 53.7 %layer.1.packed_ref = bf16[16,512]{1,0:T(8,128)(2,1)S(1)} custom-call(bf16[16,4096]{1,0:T(8,128)(2,1)} %tokens_h.1, f32[1,4096]{1,0:T(1,128)} %bitcast.8, bf16[256,128]{1,0:T(8,128)(2,1)} %wq_h.1, bf16[256,128]{1,0:T(8,128)(2,1)} %wk_h.1, bf16[256,128]{1,0:T(8,128)(2,1)} %wv_h.1, f32[1]{0:T(128)S(6)} %copy.22.lam_h, f32[1,128]{1,0:T(1,128)} %bitcast.12, ...), custom_call_target="tpu_custom_call" | custom-call | tf_op jit(solution)/shard_map/layer/pallas_call | solution.py:593
  55.0 0.6 %unpack.1 = (bf16[16,256]{1,0:T(8,128)(2,1)}, bf16[16,128]{1,0:T(8,128)(2,1)}, bf16[16,128]{1,0:T(8,128)(2,1)}) custom-call(bf16[16,512]{1,0:T(8,128)(2,1)S(1)} %layer.1.packed_ref), custom_call_target="tpu_custom_call" | custom-call | tf_op jit(solution)/shard_map/unpack/pallas_call | solution.py:602

commit v4 on v3

--- a/solution.py
+++ b/solution.py
@@ -490,15 +490,14 @@
             send_h[pl.ds(2 * r + h, n, stride=8), :] = expert_out[r * n : (r + 1) * n, h * 128 : (h + 1) * 128]
     recv_h[pl.ds(pl.multiple_of(ep * 8, 8), 4), :] = send_h[pl.ds(pl.multiple_of(ep * 8, 8), 4), :]
     h_start(ep_peers)
+    for sent in (a_sent, b_sent, e_sent, h_sent):
+        lax.fori_loop(1, n, sent, 0)
+    for copy in outgoing:
+        copy.wait_send()
     wait_all(h_arrived)
     back = jnp.dot(shares, recv_h[...].astype(BF16), preferred_element_type=F32)
     routed = [sum(back[(3 * h + i) * seqs : (3 * h + i + 1) * seqs] for i in range(3)) for h in range(2)]
     out_ref[:, :cols] = (resid + jnp.concatenate(routed, axis=1)).astype(BF16)
-
-    for sent in (a_sent, b_sent, e_sent, h_sent):
-        lax.fori_loop(1, n, sent, 0)
-    for copy in outgoing:
-        copy.wait_send()
 
 
 def unpack_kernel(packed_ref, mixed_ref, fresh_k_ref, fresh_v_ref, sems):

time: 55.8 us -> 54.9 us (0.984)
  Pallas kernels: 54.4 us -> 53.5 us
    pallas_call x1, Pallas kernels: 53.7 us -> 52.9 us  [on_device(): pl.pallas_call(functools.partial(layer_kernel, n), out_shape=pltpu.VMEM((...]
where the time goes in v4:
time: 54.9 us; the launch traced here: 54.8 us
  Pallas kernels  53.5 us (97%)
  between operations  1.29 us (2%)
    pallas_call x1, Pallas kernels, on_device(): pl.pallas_call(functools.partial(layer_kernel, n), out_shape=pltpu.VMEM((...  52.9 us

profile of v4, /device:TPU:8, one launch (start us, length us, event | category | flops | bytes accessed | tf_op | source)
XLA Modules:
  0.0 54.8 jit_solution(8714082966183892703)
XLA Ops:
  1.3 52.9 %layer.1.packed_ref = bf16[16,512]{1,0:T(8,128)(2,1)S(1)} custom-call(bf16[16,4096]{1,0:T(8,128)(2,1)} %tokens_h.1, f32[1,4096]{1,0:T(1,128)} %bitcast.8, bf16[256,128]{1,0:T(8,128)(2,1)} %wq_h.1, bf16[256,128]{1,0:T(8,128)(2,1)} %wk_h.1, bf16[256,128]{1,0:T(8,128)(2,1)} %wv_h.1, f32[1]{0:T(128)S(6)} %copy.22.lam_h, f32[1,128]{1,0:T(1,128)} %bitcast.12, ...), custom_call_target="tpu_custom_call" | custom-call | tf_op jit(solution)/shard_map/layer/pallas_call | solution.py:592
  54.2 0.6 %unpack.1 = (bf16[16,256]{1,0:T(8,128)(2,1)}, bf16[16,128]{1,0:T(8,128)(2,1)}, bf16[16,128]{1,0:T(8,128)(2,1)}) custom-call(bf16[16,512]{1,0:T(8,128)(2,1)S(1)} %layer.1.packed_ref), custom_call_target="tpu_custom_call" | custom-call | tf_op jit(solution)/shard_map/unpack/pallas_call | solution.py:601

commit v5 on v4

--- a/solution.py
+++ b/solution.py
@@ -389,6 +389,8 @@
     send_c[...] = (term_own[...] + term_in[...].astype(F32)).astype(BF16)
     c_wait = along_z(2, lambda i: send_c.at[i], recv_c)
     recv_c[chip] = send_c[chip]
+    for sent in (a_sent, b_sent):
+        lax.fori_loop(1, n, sent, 0)
     c_wait()
     attn_sum = jnp.sum(recv_c[...].astype(F32), axis=0)
     own_cols = pl.ds(pl.multiple_of(tp * cols, cols), cols)
@@ -490,7 +492,7 @@
             send_h[pl.ds(2 * r + h, n, stride=8), :] = expert_out[r * n : (r + 1) * n, h * 128 : (h + 1) * 128]
     recv_h[pl.ds(pl.multiple_of(ep * 8, 8), 4), :] = send_h[pl.ds(pl.multiple_of(ep * 8, 8), 4), :]
     h_start(ep_peers)
-    for sent in (a_sent, b_sent, e_sent, h_sent):
+    for sent in (e_sent, h_sent):
         lax.fori_loop(1, n, sent, 0)
     for copy in outgoing:
         copy.wait_send()

time: 54.9 us -> 54.9 us (level)
  no operation moved by 1% of the time
where the time goes in v5:
time: 54.9 us; the launch traced here: 54.8 us
  Pallas kernels  53.5 us (97%)
  between operations  1.29 us (2%)
    pallas_call x1, Pallas kernels, on_device(): pl.pallas_call(functools.partial(layer_kernel, n), out_shape=pltpu.VMEM((...  52.9 us

profile of v5, /device:TPU:8, one launch (start us, length us, event | category | flops | bytes accessed | tf_op | source)
XLA Modules:
  0.0 54.8 jit_solution(12202976946876760548)
XLA Ops:
  1.3 52.9 %layer.1.packed_ref = bf16[16,512]{1,0:T(8,128)(2,1)S(1)} custom-call(bf16[16,4096]{1,0:T(8,128)(2,1)} %tokens_h.1, f32[1,4096]{1,0:T(1,128)} %bitcast.8, bf16[256,128]{1,0:T(8,128)(2,1)} %wq_h.1, bf16[256,128]{1,0:T(8,128)(2,1)} %wk_h.1, bf16[256,128]{1,0:T(8,128)(2,1)} %wv_h.1, f32[1]{0:T(128)S(6)} %copy.22.lam_h, f32[1,128]{1,0:T(1,128)} %bitcast.12, ...), custom_call_target="tpu_custom_call" | custom-call | tf_op jit(solution)/shard_map/layer/pallas_call | solution.py:594
  54.2 0.6 %unpack.1 = (bf16[16,256]{1,0:T(8,128)(2,1)}, bf16[16,128]{1,0:T(8,128)(2,1)}, bf16[16,128]{1,0:T(8,128)(2,1)}) custom-call(bf16[16,512]{1,0:T(8,128)(2,1)S(1)} %layer.1.packed_ref), custom_call_target="tpu_custom_call" | custom-call | tf_op jit(solution)/shard_map/unpack/pallas_call | solution.py:603
